TPU v7x, 32 devices: a whole 2x2x4 slice. The times are simulated.
32 devices in a mesh: grp: 2 (over y), ep: 4 (over z), tp: 4 (over x, core).
Axes of the slice: x: 2, y: 2, z: 4, core: 2. Of those that a mesh axis runs over, the one named last changes fastest.
Arguments:
- memory_query_rows: bfloat16 [1024, 1024], P(('grp', 'ep'), 'tp'), parts along dimension 0, may hold values from -6 to 6
- memory_key_rows: bfloat16 [1024, 1024], P(('grp', 'ep'), 'tp'), parts along dimension 0, may hold values from -6 to 6
- memory_value_rows: bfloat16 [1024, 1024], P(('grp', 'ep'), 'tp'), parts along dimension 0, may hold values from -6 to 6
- input_gate_log: float32 [8, 1024], P('tp', ('grp', 'ep')), parts along dimension 1, may hold values from -4 to 300
- forget_gate_logits: float32 [8, 1024], P('tp', ('grp', 'ep')), parts along dimension 1
- forget_log_extra: float32 [8, 1024], P('tp', ('grp', 'ep')), parts along dimension 1, may hold values from -1.5 to 0
- memory_output_weight: bfloat16 [1024, 2048], P(None, 'tp'), may hold values from -0.1875 to 0.1875
- second_batch_tokens: bfloat16 [4096, 2048], P(('grp', 'ep', 'tp')), parts along dimension 0, may hold values from -6 to 6
- expert_norm_gain: float32 [2048], replicated, may hold values from 0.1 to 1.9
- routing_expert_index: int32 [4096, 2], P(('grp', 'ep', 'tp')), parts along dimension 0, may hold values from 0 to 3, all different within a row; in each aligned block of 128 rows (0 to 127, 128 to 255, ...) at most 80 rows name the same one
- routing_expert_weight: float32 [4096, 2], P(('grp', 'ep', 'tp')), parts along dimension 0, may hold values from 0.2 to 1
- expert_gate_matrix: bfloat16 [4, 2048, 3584], P('ep', None, 'tp'), may hold values from -0.125 to 0.125
- expert_up_matrix: bfloat16 [4, 2048, 3584], P('ep', None, 'tp'), may hold values from -0.125 to 0.125
- expert_down_matrix: bfloat16 [4, 3584, 2048], P('ep', 'tp'), may hold values from -0.09375 to 0.09375
Outputs:
- mixed_out: bfloat16 [1024, 2048], P(('grp', 'ep'), 'tp'), parts along dimension 0
- expert_out: bfloat16 [4096, 2048], P(('grp', 'ep', 'tp')), parts along dimension 0
There are 2 independent parts, one for each index of `grp`. A program takes and returns all parts, laid end to end along the dimension named above; an argument that names none is the same for every part. Nothing has to cross between parts.
Inputs may be any that keep to these rules, and one draw needn't show every extreme that they name: `routing_expert_index`: within the rows of one device no expert is named by more than 80 rows, a bound that some block reaches; the 2 experts of a row differ.
All inputs are finite; a program needn't handle non-finite values.
Results may differ from a plain program's by a relative error of at most 0.012.
The roundings to bfloat16 on the way count: a program that leaves them out, or rounds other values in their place, can miss the bound.
Values may be sent and summed in bfloat16 or wider, within the bound.
No kernel may reach another device: no remote copies, remote signals or barrier semaphores. Data moves between devices by JAX's collectives and lax.ppermute only.
A program may use at most 128 MiB of HBM per device.

v0:
```python
import jax
import jax.numpy as jnp
from jax import lax
from jax.experimental import pallas as pl
from jax.experimental.pallas import tpu as pltpu
from jax.sharding import PartitionSpec as P

DH = 128
TOP = 2
BLOCK = 128


neg_big = -1e30
rms_eps = 1e-06
highest = lax.Precision.HIGHEST


def entering(part, axis, combine, identity):
    place = lax.axis_index(axis)
    gathered = jax.tree.map(lambda a: lax.all_gather(a, axis), part)
    state = jax.tree.map(lambda a, e: jnp.zeros_like(a) + jnp.asarray(e, a.dtype), part, identity)

    def one(turn, state):
        return combine(
            state, jax.tree.map(lambda a: lax.dynamic_index_in_dim(a, turn, 0, False), gathered)
        )

    return lax.fori_loop(0, place, one, state)


def state_update(state_in, inputs, cumulative):
    memory, normer, stabilizer = state_in
    key_rows, values, in_gate, _ = inputs
    block_total = cumulative[:, -1]
    weights = block_total[:, None] - cumulative + in_gate
    new_stab = jnp.maximum(block_total + stabilizer, jnp.max(weights, axis=-1))
    scaled = jnp.exp(weights - new_stab[:, None])
    retained = jnp.exp(block_total + stabilizer - new_stab)
    weighted_keys = scaled[:, :, None] * key_rows
    memory = retained[:, None, None] * memory + jnp.einsum(
        "hsd,hse->hde", weighted_keys, values, precision=highest
    )
    normer = retained[:, None] * normer + jnp.sum(weighted_keys, axis=1)
    return (memory, normer, new_stab)


def block_step(state_in, inputs, cumulative):
    memory, normer, stabilizer = state_in
    queries, key_rows, values, in_gate, _ = inputs
    length = queries.shape[1]
    causal = jnp.tril(jnp.ones((length, length), dtype=bool))
    decays = jnp.where(
        causal, cumulative[:, :, None] - cumulative[:, None, :] + in_gate[:, None, :], -jnp.inf
    )
    carried_max = cumulative + stabilizer[:, None]
    row_max = jnp.maximum(jnp.max(decays, axis=-1), carried_max)
    scores = jnp.einsum("htd,hsd->hts", queries, key_rows, precision=highest) * jnp.exp(
        decays - row_max[:, :, None]
    )
    carried = jnp.exp(carried_max - row_max)
    numerator = carried[:, :, None] * jnp.einsum(
        "htd,hde->hte", queries, memory, precision=highest
    ) + jnp.einsum("hts,hse->hte", scores, values, precision=highest)
    denominator = carried * jnp.einsum("htd,hd->ht", queries, normer, precision=highest) + jnp.sum(
        scores, axis=-1
    )
    return numerator / jnp.maximum(jnp.abs(denominator), jnp.exp(-row_max))[:, :, None]


def join_states(earlier, later, total_late):
    mem_early, norm_early, stab_early = earlier
    mem_late, norm_late, stab_late = later
    stabilizer = jnp.maximum(total_late + stab_early, stab_late)
    early_scale = jnp.exp(total_late + stab_early - stabilizer)
    late_scale = jnp.exp(stab_late - stabilizer)
    memory = early_scale[:, None, None] * mem_early + late_scale[:, None, None] * mem_late
    normer = early_scale[:, None] * norm_early + late_scale[:, None] * norm_late
    return (memory, normer, stabilizer)


def join_totals(earlier, later):
    joined = join_states(earlier[:3], later[:3], later[3])
    return joined + (earlier[3] + later[3],)


def split_blocks(row_block, heads):
    count = row_block.shape[0] // BLOCK
    return row_block.astype(jnp.float32).reshape(count, BLOCK, heads, -1).transpose(0, 2, 1, 3)


def gate_blocks(gate_rows):
    heads = gate_rows.shape[0]
    return gate_rows.reshape(heads, -1, BLOCK).transpose(1, 0, 2)


def swap(rows, axis, bit):
    size = lax.axis_size(axis)
    return lax.ppermute(rows, axis, [(i, i ^ bit) for i in range(size)])


def tp_bits():
    size = lax.axis_size("tp")
    bits = []
    while size > 1:
        size //= 2
        bits.append(size)
    return bits


def gather_columns(rows):
    place = lax.axis_index("tp")
    for bit in reversed(tp_bits()):
        other = swap(rows, "tp", bit)
        upper = (place & bit) != 0
        rows = jnp.concatenate(
            [jnp.where(upper, other, rows), jnp.where(upper, rows, other)], axis=1
        )
    return rows


def memory_branch(
    memory_query_rows,
    memory_key_rows,
    memory_value_rows,
    input_gate_log,
    forget_gate_logits,
    forget_log_extra,
    memory_output_weight,
):
    heads_local, positions = input_gate_log.shape
    queries = split_blocks(memory_query_rows, heads_local)
    key_rows = split_blocks(memory_key_rows, heads_local) * DH ** (-0.5)
    values = split_blocks(memory_value_rows, heads_local)
    in_gate = gate_blocks(input_gate_log)
    forget_log_value = jax.nn.log_sigmoid(forget_gate_logits) + forget_log_extra
    forget = gate_blocks(forget_log_value)
    upto = jnp.triu(jnp.ones((BLOCK, BLOCK), jnp.float32))
    cumulative = jnp.einsum("bhs,st->bht", forget, upto, precision=highest)
    zero_memory = jnp.zeros((heads_local, DH, DH), jnp.float32)
    zero_normer = jnp.zeros((heads_local, DH), jnp.float32)
    low_stab = jnp.full((heads_local,), neg_big, jnp.float32)
    count = positions // BLOCK
    state = (zero_memory, zero_normer, low_stab)
    for b in range(count):
        state = state_update(state, (key_rows[b], values[b], in_gate[b], forget[b]), cumulative[b])
    totals = jnp.sum(cumulative[:, :, -1], axis=0)
    identity = (zero_memory, zero_normer, low_stab, jnp.zeros((heads_local,), jnp.float32))
    mem_prior, norm_prior, stab_prior, total_prior = entering(
        state + (totals,), "ep", join_totals, identity
    )
    stab_in = jnp.maximum(total_prior, stab_prior)
    factor = jnp.exp(stab_prior - stab_in)
    incoming = (factor[:, None, None] * mem_prior, factor[:, None] * norm_prior, stab_in)
    outputs = []
    for b in range(count):
        block = (queries[b], key_rows[b], values[b], in_gate[b], forget[b])
        outputs.append(block_step(incoming, block, cumulative[b]))
        if b + 1 < count:
            incoming = state_update(incoming, block[1:], cumulative[b])
    memory_rows = (
        jnp.stack(outputs).transpose(0, 2, 1, 3).reshape(positions, -1).astype(jnp.bfloat16)
    )
    mixed = jnp.dot(
        gather_columns(memory_rows), memory_output_weight, preferred_element_type=jnp.float32
    )
    return mixed.astype(jnp.bfloat16)


def split_terms(array):
    high = array.astype(jnp.bfloat16)
    return high, (array - high.astype(jnp.float32)).astype(jnp.bfloat16)


def wide_dot(left, right):
    high, low = split_terms(left)
    both = jnp.dot(
        jnp.concatenate([high, low], axis=0), right, preferred_element_type=jnp.float32
    )
    return both[: left.shape[0]] + both[left.shape[0] :]


def local_kernel(query, key, value, gate, logits, extra, local, after, inside, columns):
    heads = gate.shape[0]
    size = query.shape[0]
    scale = DH ** (-0.5)
    raw = logits[...]
    forget = jnp.minimum(raw, 0.0) - jnp.log1p(jnp.exp(-jnp.abs(raw))) + extra[...]
    first = lax.broadcasted_iota(jnp.int32, (size, size), 0)
    second = lax.broadcasted_iota(jnp.int32, (size, size), 1)
    upto = (first <= second).astype(jnp.float32)
    cumulative = jnp.dot(forget, upto, precision=highest, preferred_element_type=jnp.float32)
    ending = cumulative[:, size - 1 : size] - cumulative + gate[...]
    peak = jnp.max(ending, axis=1, keepdims=True)
    grow = jnp.exp(ending - peak)
    blank = jnp.zeros((size - 2 * heads, size), jnp.float32)
    turned = jnp.concatenate([cumulative, grow, blank], axis=0).T
    notes = [jnp.zeros((size, size - 3 * heads), jnp.float32)]
    for h in range(heads):
        span = slice(h * DH, (h + 1) * DH)
        queries = query[:, span]
        keys = key[:, span]
        values = value[:, span]
        keys_f = keys.astype(jnp.float32) * scale
        weighted = keys_f.T * grow[h : h + 1, :]
        memory = wide_dot(weighted, values)
        normer = jnp.sum(keys_f * turned[:, heads + h : heads + h + 1], axis=0, keepdims=True)
        total = cumulative[h : h + 1, size - 1 : size]
        stab = peak[h : h + 1, :]
        later = jnp.maximum(total, stab)
        ratio = jnp.exp(stab - later)
        local[h, 0:DH, :] = memory
        local[h, DH : DH + 1, :] = normer
        local[h, DH + 1 : DH + 2, :] = jnp.broadcast_to(stab, (1, DH))
        local[h, DH + 2 : DH + 3, :] = jnp.broadcast_to(total, (1, DH))
        after[h, 0:DH, :] = memory * ratio
        after[h, DH : DH + 1, :] = normer * ratio
        after[h, DH + 1 : DH + 2, :] = jnp.broadcast_to(later, (1, DH))
        column = turned[:, h : h + 1]
        decays = column - cumulative[h : h + 1, :] + gate[h : h + 1, :]
        decays = jnp.where(second <= first, decays, -jnp.inf)
        row_max = jnp.max(decays, axis=1, keepdims=True)
        scores = lax.dot_general(
            queries, keys, (((1,), (1,)), ((), ())), preferred_element_type=jnp.float32
        )
        scores = scores * scale * jnp.exp(decays - row_max)
        inside[:, span] = wide_dot(scores, values)
        notes = notes[:-1] + [column, row_max, jnp.sum(scores, axis=1, keepdims=True)] + notes[-1:]
    columns[...] = jnp.concatenate(notes, axis=1)


def join_kernel(local, *refs):
    earlier = refs[:-1]
    after = refs[-1]
    for h in range(local.shape[0]):
        entering = sum(part[h] for part in earlier)
        stab = entering[DH + 1 : DH + 2, :] + local[h, DH + 2 : DH + 3, :]
        late = local[h, DH + 1 : DH + 2, :]
        later = jnp.maximum(stab, late)
        keep = jnp.exp(stab - later)
        grow = jnp.exp(late - later)
        after[h, 0 : DH + 1, :] = entering[0 : DH + 1, :] * keep + local[h, 0 : DH + 1, :] * grow
        after[h, DH + 1 : DH + 2, :] = later


def output_kernel(query, inside, columns, *refs):
    earlier = refs[:-1]
    out = refs[-1]
    for h in range(earlier[0].shape[0]):
        span = slice(h * DH, (h + 1) * DH)
        entering = sum(part[h] for part in earlier)
        queries = query[:, span]
        high, low = split_terms(entering[0:DH, :])
        carried = jnp.dot(queries, high, preferred_element_type=jnp.float32) + jnp.dot(
            queries, low, preferred_element_type=jnp.float32
        )
        normed = jnp.sum(
            queries.astype(jnp.float32) * entering[DH : DH + 1, :], axis=1, keepdims=True
        )
        arrived = columns[:, 3 * h : 3 * h + 1] + entering[DH + 1 : DH + 2, 0:1]
        row_max = columns[:, 3 * h + 1 : 3 * h + 2]
        top = jnp.maximum(row_max, arrived)
        outer = jnp.exp(arrived - top)
        inner = jnp.exp(row_max - top)
        below = outer * normed + inner * columns[:, 3 * h + 2 : 3 * h + 3]
        above = outer * carried + inner * inside[:, span]
        out[:, span] = (above / jnp.maximum(jnp.abs(below), jnp.exp(-top))).astype(jnp.bfloat16)


def mixed_kernel(place, own, across, beside, corner, weight, out):
    width = own.shape[1]
    total = jnp.zeros(out.shape, jnp.float32)
    for mask, part in ((0, own), (2, across), (1, beside), (3, corner)):
        rows = pl.ds(pl.multiple_of((place[0] ^ mask) * width, width), width)
        total += jnp.dot(part[...], weight[rows, :], preferred_element_type=jnp.float32)
    out[...] = total.astype(jnp.bfloat16)


def memory_pairs(
    memory_query_rows,
    memory_key_rows,
    memory_value_rows,
    input_gate_log,
    forget_gate_logits,
    forget_log_extra,
    memory_output_weight,
):
    heads = input_gate_log.shape[0]
    size, width = memory_query_rows.shape
    vmem = pl.BlockSpec(memory_space=pltpu.VMEM)
    params = pltpu.CompilerParams(vmem_limit_bytes=8 * 1024 * 1024)
    packed = jax.ShapeDtypeStruct((heads, DH + 8, DH), jnp.float32)
    local, after, inside, columns = pl.pallas_call(
        local_kernel,
        in_specs=[vmem] * 6,
        out_specs=[vmem] * 4,
        out_shape=[
            packed,
            packed,
            jax.ShapeDtypeStruct((size, width), jnp.float32),
            jax.ShapeDtypeStruct((size, size), jnp.float32),
        ],
        compiler_params=params,
    )(
        memory_query_rows,
        memory_key_rows,
        memory_value_rows,
        input_gate_log,
        forget_gate_logits,
        forget_log_extra,
    )
    earlier = []
    hops = lax.axis_size("ep") - 1
    for hop in range(hops):
        if hop:
            after = pl.pallas_call(
                join_kernel,
                in_specs=[vmem] * (1 + hop),
                out_specs=vmem,
                out_shape=packed,
                compiler_params=params,
            )(local, *earlier)
        earlier.append(lax.ppermute(after, "ep", [(hop, hop + 1)]))
    own = pl.pallas_call(
        output_kernel,
        in_specs=[vmem] * (3 + hops),
        out_specs=vmem,
        out_shape=jax.ShapeDtypeStruct((size, width), jnp.bfloat16),
        compiler_params=params,
    )(memory_query_rows, inside, columns, *earlier)
    across = swap(own, "tp", 2)
    beside = swap(own, "tp", 1)
    corner = swap(across, "tp", 1)
    place = lax.axis_index("tp").astype(jnp.int32).reshape(1)
    return pl.pallas_call(
        mixed_kernel,
        in_specs=[pl.BlockSpec(memory_space=pltpu.SMEM)] + [vmem] * 5,
        out_specs=vmem,
        out_shape=jax.ShapeDtypeStruct((size, memory_output_weight.shape[1]), jnp.bfloat16),
        compiler_params=params,
    )(place, own, across, beside, corner, memory_output_weight)


def expert_part(rows, gate_weight, up_weight, down_weight):
    gate_act = jnp.dot(rows, gate_weight, preferred_element_type=jnp.float32)
    up_act = jnp.dot(rows, up_weight, preferred_element_type=jnp.float32)
    hidden = (jax.nn.silu(gate_act) * up_act).astype(jnp.bfloat16)
    return jnp.dot(hidden, down_weight, preferred_element_type=jnp.float32)


def in_hbm(array):
    return pltpu.with_memory_space_constraint(array, pltpu.HBM)


def prepare_kernel(count, place, *refs):
    sources = refs[:4]
    table = refs[4]
    outgoing = refs[5 : 5 + count]
    tokens, gain, ids, shares, sems = refs[5 + count :]
    copies = [
        pltpu.make_async_copy(source, target, sems.at[n])
        for n, (source, target) in enumerate(
            zip(sources, (tokens, gain, ids, shares), strict=True)
        )
    ]
    for copy in copies:
        copy.start()
    for copy in copies:
        copy.wait()
    tok_rows = tokens.shape[0]
    capacity = outgoing[0].shape[0]
    values = tokens[...].astype(jnp.float32)
    scale = lax.rsqrt(jnp.mean(values * values, axis=1, keepdims=True) + rms_eps)
    normed = (values * scale * gain[...]).astype(jnp.bfloat16)
    named = []
    weighted = []
    for k in range(count):
        hit = [ids[c : c + 1, :] == (place[0] ^ k) for c in range(TOP)]
        named.append(sum(h.astype(jnp.float32) for h in hit))
        weighted.append(sum(jnp.where(h, shares[c : c + 1, :], 0.0) for c, h in enumerate(hit)))
    half = tok_rows // 2
    blank = jnp.zeros((half - count, tok_rows), jnp.float32)
    named = jnp.concatenate(named + [blank], axis=0)
    upto = lax.broadcasted_iota(jnp.int32, (tok_rows, tok_rows), 0) <= lax.broadcasted_iota(
        jnp.int32, (tok_rows, tok_rows), 1
    )
    ranks = jnp.dot(
        named.astype(jnp.bfloat16),
        upto.astype(jnp.bfloat16),
        preferred_element_type=jnp.float32,
    )
    slots = jnp.where(named > 0.5, ranks - 1.0, -1.0)
    table[...] = jnp.concatenate([slots] + weighted + [blank], axis=0).T
    spots = lax.broadcasted_iota(jnp.int32, (capacity, tok_rows), 0).astype(jnp.float32)
    for k in reversed(range(count)):
        placing = (spots == slots[k : k + 1, :]).astype(jnp.bfloat16)
        outgoing[k][...] = jnp.dot(
            placing, normed, preferred_element_type=jnp.float32
        ).astype(jnp.bfloat16)


def prepare(tokens, gain, routing_expert_index, routing_expert_weight, count, capacity):
    tok_rows, width = tokens.shape
    vmem = pl.BlockSpec(memory_space=pltpu.VMEM)
    place = lax.axis_index("ep").astype(jnp.int32).reshape(1)
    return pl.pallas_call(
        lambda *refs: prepare_kernel(count, *refs),
        in_specs=[pl.BlockSpec(memory_space=pltpu.SMEM)]
        + [pl.BlockSpec(memory_space=pltpu.HBM)] * 4,
        out_specs=[vmem] * (count + 1),
        out_shape=[jax.ShapeDtypeStruct((tok_rows, tok_rows), jnp.float32)]
        + [jax.ShapeDtypeStruct((capacity, width), jnp.bfloat16)] * count,
        scratch_shapes=[
            pltpu.VMEM((tok_rows, width), jnp.bfloat16),
            pltpu.VMEM((1, width), jnp.float32),
            pltpu.VMEM((TOP, tok_rows), jnp.int32),
            pltpu.VMEM((TOP, tok_rows), jnp.float32),
            pltpu.SemaphoreType.DMA((4,)),
        ],
        compiler_params=pltpu.CompilerParams(vmem_limit_bytes=16 * 1024 * 1024),
    )(
        place,
        in_hbm(tokens),
        in_hbm(gain.reshape(1, width)),
        in_hbm(routing_expert_index.T),
        in_hbm(routing_expert_weight.T),
    )


def combine_kernel(count, table, *refs):
    returned = refs[: count + 1]
    out, stacked = refs[count + 1 :]
    tok_rows = out.shape[0]
    half = tok_rows // 2
    capacity = returned[0].shape[0]
    local = returned[0][...].astype(jnp.float32) + returned[count][...].astype(jnp.float32)
    stacked[0:capacity, :] = local.astype(jnp.bfloat16)
    for k in range(1, count):
        stacked[k * capacity : (k + 1) * capacity, :] = returned[k][...]
    spots = lax.broadcasted_iota(jnp.int32, (tok_rows, count * capacity), 1).astype(jnp.float32)
    weights = jnp.zeros((tok_rows, count * capacity), jnp.float32)
    for k in range(count):
        slot = table[:, k : k + 1]
        aim = jnp.where(slot >= 0.0, slot + float(k * capacity), -1.0)
        weights = jnp.where(spots == aim, table[:, half + k : half + k + 1], weights)
    high = weights.astype(jnp.bfloat16)
    low = (weights - high.astype(jnp.float32)).astype(jnp.bfloat16)
    both = jnp.dot(
        jnp.concatenate([high, low], axis=0), stacked[...], preferred_element_type=jnp.float32
    )
    out[...] = (both[:tok_rows] + both[tok_rows:]).astype(jnp.bfloat16)


def combine_rows(table, returned):
    count = len(returned) - 1
    capacity, width = returned[0].shape
    vmem = pl.BlockSpec(memory_space=pltpu.VMEM)
    return pl.pallas_call(
        lambda *refs: combine_kernel(count, *refs),
        in_specs=[vmem] * (count + 2),
        out_specs=vmem,
        out_shape=jax.ShapeDtypeStruct((table.shape[0], width), jnp.bfloat16),
        scratch_shapes=[pltpu.VMEM((count * capacity, width), jnp.bfloat16)],
        compiler_params=pltpu.CompilerParams(vmem_limit_bytes=16 * 1024 * 1024),
    )(table, *returned)


def expert_kernel(*refs):
    pieces = refs[:4]
    gate, up, down = refs[4:7]
    outs = refs[7:10]
    rows, hidden, gate_here, up_here, down_here, sems = refs[10:]
    copies = [
        pltpu.make_async_copy(gate.at[0], gate_here, sems.at[0]),
        pltpu.make_async_copy(up.at[0], up_here, sems.at[1]),
        pltpu.make_async_copy(down.at[0], down_here, sems.at[2]),
    ]
    for copy in copies:
        copy.start()
    at = 0
    for piece in pieces:
        rows[at : at + piece.shape[0], :] = piece[...]
        at += piece.shape[0]
    copies[0].wait()
    gate_act = jnp.dot(rows[...], gate_here[...], preferred_element_type=jnp.float32)
    copies[1].wait()
    up_act = jnp.dot(rows[...], up_here[...], preferred_element_type=jnp.float32)
    hidden[...] = (gate_act / (1.0 + jnp.exp(-gate_act)) * up_act).astype(jnp.bfloat16)
    copies[2].wait()
    parts = jnp.dot(hidden[...], down_here[...], preferred_element_type=jnp.float32)
    at = 0
    for out in outs:
        out[...] = parts[at : at + out.shape[0]].astype(jnp.bfloat16)
        at += out.shape[0]


def expert_rows(pieces, gate, up, down):
    count, width = pieces[0].shape
    inner = gate.shape[-1]
    vmem = pl.BlockSpec(memory_space=pltpu.VMEM)
    hbm = pl.BlockSpec(memory_space=pltpu.HBM)
    return pl.pallas_call(
        expert_kernel,
        in_specs=[vmem] * 4 + [hbm] * 3,
        out_specs=[vmem] * 3,
        out_shape=[
            jax.ShapeDtypeStruct((n * count, width), jnp.bfloat16) for n in (1, 1, 2)
        ],
        scratch_shapes=[
            pltpu.VMEM((4 * count, width), jnp.bfloat16),
            pltpu.VMEM((4 * count, inner), jnp.bfloat16),
            pltpu.VMEM((width, inner), jnp.bfloat16),
            pltpu.VMEM((width, inner), jnp.bfloat16),
            pltpu.VMEM((inner, width), jnp.bfloat16),
            pltpu.SemaphoreType.DMA((3,)),
        ],
        compiler_params=pltpu.CompilerParams(vmem_limit_bytes=32 * 1024 * 1024),
        cost_estimate=pl.CostEstimate(
            flops=24 * count * width * inner,
            bytes_accessed=6 * width * inner,
            transcendentals=4 * count * inner,
        ),
    )(*pieces, *(in_hbm(w) for w in (gate, up, down)))


def added(first, second):
    total = first.astype(jnp.float32) + second.astype(jnp.float32)
    return total.astype(jnp.bfloat16)


def near_sum_kernel(keep, send, pair, kept, sent):
    rows = keep.shape[0]
    kept[...] = added(keep[...], pair[:rows])
    sent[...] = added(send[...], pair[rows:])


def far_sum_kernel(keep, other, out):
    out[...] = added(keep[...], other[...])


def sums(kernel, outputs, *rows):
    vmem = pl.BlockSpec(memory_space=pltpu.VMEM)
    return pl.pallas_call(
        kernel,
        in_specs=[vmem] * len(rows),
        out_specs=[vmem] * outputs,
        out_shape=[jax.ShapeDtypeStruct(rows[0].shape, jnp.bfloat16)] * outputs,
        compiler_params=pltpu.CompilerParams(vmem_limit_bytes=8 * 1024 * 1024),
    )(*rows)


def expert_pairs(
    second_batch_tokens,
    expert_norm_gain,
    routing_expert_index,
    routing_expert_weight,
    gate,
    up,
    down,
):
    experts = lax.axis_size("ep")
    tok_rows = second_batch_tokens.shape[0]
    capacity = max(2, 5 * tok_rows * TOP // (4 * experts))
    table, *outgoing = prepare(
        second_batch_tokens,
        expert_norm_gain,
        routing_expert_index,
        routing_expert_weight,
        experts,
        capacity,
    )
    far, near = 2, 1
    returned = [None] * experts + [None]
    for k in reversed(range(experts)):
        own = swap(outgoing[k], "ep", k) if k else outgoing[k]
        across = swap(own, "tp", far)
        beside = swap(own, "tp", near)
        corner = swap(across, "tp", near)
        pieces = (own, across, beside, corner)
        keep, send, pair = expert_rows(pieces, gate, up, down)
        pair = swap(pair, "tp", near)
        keep, send = sums(near_sum_kernel, 2, keep, send, pair)
        other = swap(send, "tp", far)
        if k:
            total = sums(far_sum_kernel, 1, keep, other)[0]
            returned[k] = swap(total, "ep", k)
        else:
            returned[0] = keep
            returned[experts] = other
    return combine_rows(table, returned)


def expert_branch(
    second_batch_tokens,
    expert_norm_gain,
    routing_expert_index,
    routing_expert_weight,
    gate,
    up,
    down,
):
    tok_rows = second_batch_tokens.shape[0]
    experts = lax.axis_size("ep")
    capacity = max(2, 5 * tok_rows * TOP // (4 * experts))
    tokens_f = second_batch_tokens.astype(jnp.float32)
    normed = (
        tokens_f
        * lax.rsqrt(jnp.mean(tokens_f * tokens_f, axis=1, keepdims=True) + rms_eps)
        * expert_norm_gain
    ).astype(jnp.bfloat16)
    ids = jnp.arange(experts, dtype=jnp.int32)
    hits = routing_expert_index[:, :, None] == ids[None, None, :]
    named = jnp.any(hits, axis=1)
    share = jnp.sum(jnp.where(hits, routing_expert_weight[:, :, None], 0.0), axis=1)
    upto = jnp.tril(jnp.ones((tok_rows, tok_rows), jnp.bfloat16))
    ranks = jnp.dot(upto, named.astype(jnp.bfloat16), preferred_element_type=jnp.float32)
    slot = jnp.where(named, ranks.astype(jnp.int32) - 1, -1)
    spots = jnp.arange(capacity, dtype=jnp.int32)
    placing = (slot.T[:, None, :] == spots[None, :, None]).astype(jnp.bfloat16)
    combine = jnp.where(slot[:, :, None] == spots[None, None, :], share[:, :, None], 0.0)
    outgoing = jnp.dot(
        placing.reshape(experts * capacity, tok_rows),
        normed,
        preferred_element_type=jnp.float32,
    ).astype(jnp.bfloat16)
    arrived = lax.all_to_all(outgoing, "ep", split_axis=0, concat_axis=0, tiled=True)
    row_block = lax.all_gather(arrived, "tp", axis=0, tiled=True)
    terms = expert_part(row_block, gate[0], up[0], down[0]).astype(jnp.bfloat16)
    summed = lax.psum_scatter(terms, "tp", scatter_dimension=0, tiled=True)
    returned = lax.all_to_all(summed, "ep", split_axis=0, concat_axis=0, tiled=True)
    combine = combine.reshape(tok_rows, experts * capacity)
    high = combine.astype(jnp.bfloat16)
    low = (combine - high.astype(jnp.float32)).astype(jnp.bfloat16)
    both = jnp.dot(
        jnp.concatenate([high, low], axis=0), returned, preferred_element_type=jnp.float32
    )
    return (both[:tok_rows] + both[tok_rows:]).astype(jnp.bfloat16)


def is_paired(experts, shards):
    return experts == 4 and shards == 4


def on_device(
    memory_query_rows,
    memory_key_rows,
    memory_value_rows,
    input_gate_log,
    forget_gate_logits,
    forget_log_extra,
    memory_output_weight,
    second_batch_tokens,
    expert_norm_gain,
    routing_expert_index,
    routing_expert_weight,
    expert_gate_matrix,
    expert_up_matrix,
    expert_down_matrix,
):
    paired = is_paired(lax.axis_size("ep"), lax.axis_size("tp"))
    paired = paired and input_gate_log.shape[1] == BLOCK
    expert_out = (expert_pairs if paired else expert_branch)(
        second_batch_tokens,
        expert_norm_gain,
        routing_expert_index,
        routing_expert_weight,
        expert_gate_matrix,
        expert_up_matrix,
        expert_down_matrix,
    )
    mixed_out = (memory_pairs if paired else memory_branch)(
        memory_query_rows,
        memory_key_rows,
        memory_value_rows,
        input_gate_log,
        forget_gate_logits,
        forget_log_extra,
        memory_output_weight,
    )
    return (mixed_out, expert_out)


def solution(mesh):
    placed = (
        P(("grp", "ep"), "tp"),
        P(("grp", "ep"), "tp"),
        P(("grp", "ep"), "tp"),
        P("tp", ("grp", "ep")),
        P("tp", ("grp", "ep")),
        P("tp", ("grp", "ep")),
        P(None, "tp"),
        P(("grp", "ep", "tp"), None),
        P(),
        P(("grp", "ep", "tp"), None),
        P(("grp", "ep", "tp"), None),
        P("ep", None, "tp"),
        P("ep", None, "tp"),
        P("ep", "tp", None),
    )
    return jax.shard_map(
        on_device,
        mesh=mesh,
        in_specs=placed,
        out_specs=(P(("grp", "ep"), "tp"), P(("grp", "ep", "tp"), None)),
        check_vma=False,
    )
```

profile of v0, /device:TPU:0, one launch (start us, length us, event | category | flops | bytes accessed | tf_op | source)
XLA Modules:
  0.0 130.3 jit_solution(17635353700810045181)
XLA Ops:
  0.6 1.8 %shard_map.154 = (f32[128,128]{1,0:T(8,128)S(1)}, bf16[80,2048]{1,0:T(8,128)(2,1)S(1)}, bf16[80,2048]{1,0:T(8,128)(2,1)S(1)}, bf16[80,2048]{1,0:T(8,128)(2,1)S(1)}, bf16[80,2048]{1,0:T(8,128)(2,1)S(1)}) custom-call(s32[1]{0:T(128)} %bitcast.1.refs_0_, bf16[128,2048]{1,0:T(8,128)(2,1)} %refs_1_.1, f32[1,2048]{1,0:T(1,128)} %bitcast.5, s32[2,128]{1,0:T(2,128)} %bitcast.6, ...), custom_call_target="tpu_custom_call" | custom-call | tf_op jit(solution)/shard_map/pallas_call | solution.py:405
  2.4 5.1 %collective-permute-start.24 = (bf16[80,2048]{1,0:T(8,128)(2,1)S(1)}, bf16[80,2048]{1,0:T(8,128)(2,1)S(1)}, u32[]{:S(2)}, u32[]{:S(2)}) collective-permute-start(bf16[80,2048]{1,0:T(8,128)(2,1)S(1)} %get-tuple-element.53), channel_id=1, source_target_pairs={{0,12},{4,8},{8,4},{12,0},{1,13},{5,9},{9,5},{13,1},{2,14},{6,10},... | collective-permute-start | bytes 983048 | tf_op jit(solution)/shard_map/ppermute | solution.py:98
  7.6 0.0 collective-permute-start.17
  7.6 8.7 %collective-permute-done.24.refs_0_ = bf16[80,2048]{1,0:T(8,128)(2,1)S(1)} collective-permute-done((bf16[80,2048]{1,0:T(8,128)(2,1)S(1)}, bf16[80,2048]{1,0:T(8,128)(2,1)S(1)}, u32[]{:S(2)}, u32[]{:S(2)}) %collective-permute-start.24) | collective-permute-done | bytes 327712 | tf_op jit(solution)/shard_map/ppermute | solution.py:98
  16.2 1.7 %collective-permute-start.25 = (bf16[80,2048]{1,0:T(8,128)(2,1)S(1)}, bf16[80,2048]{1,0:T(8,128)(2,1)S(1)}, u32[]{:S(2)}, u32[]{:S(2)}) collective-permute-start(bf16[80,2048]{1,0:T(8,128)(2,1)S(1)} %collective-permute-done.24.refs_0_), channel_id=1, source_target_pairs={{0,2},{1,3},{2,0},{3,1},{4,6},{5,7},{6,4},{7,5},{8,10},{9,11},{10,... | collective-permute-start | bytes 983048 | tf_op jit(solution)/shard_map/ppermute | solution.py:98
  17.9 13.6 %collective-permute-start.10 = (bf16[80,2048]{1,0:T(8,128)(2,1)S(1)}, bf16[80,2048]{1,0:T(8,128)(2,1)S(1)}, u32[]{:S(2)}, u32[]{:S(2)}) collective-permute-start(bf16[80,2048]{1,0:T(8,128)(2,1)S(1)} %get-tuple-element.41), channel_id=1, source_target_pairs={{0,4},{4,0},{8,12},{12,8},{1,5},{5,1},{9,13},{13,9},{2,6},{6,2},{1... | collective-permute-start | bytes 983048 | tf_op jit(solution)/shard_map/ppermute | solution.py:98
  31.5 0.0 collective-permute-start.26
  31.5 4.1 %collective-permute-done.17.refs_0_ = bf16[80,2048]{1,0:T(8,128)(2,1)S(1)} collective-permute-done((bf16[80,2048]{1,0:T(8,128)(2,1)S(1)}, bf16[80,2048]{1,0:T(8,128)(2,1)S(1)}, u32[]{:S(2)}, u32[]{:S(2)}) %collective-permute-start.17) | collective-permute-done | bytes 327712 | tf_op jit(solution)/shard_map/ppermute | solution.py:98
  35.6 1.5 %collective-permute-start.18 = (bf16[80,2048]{1,0:T(8,128)(2,1)S(1)}, bf16[80,2048]{1,0:T(8,128)(2,1)S(1)}, u32[]{:S(2)}, u32[]{:S(2)}) collective-permute-start(bf16[80,2048]{1,0:T(8,128)(2,1)S(1)} %collective-permute-done.17.refs_0_), channel_id=1, source_target_pairs={{0,2},{1,3},{2,0},{3,1},{4,6},{5,7},{6,4},{7,5},{8,10},{9,11},{10,... | collective-permute-start | bytes 983048 | tf_op jit(solution)/shard_map/ppermute | solution.py:98
  37.1 0.5 collective-permute-start.6
  37.6 4.9 %collective-permute-done.10.refs_0_ = bf16[80,2048]{1,0:T(8,128)(2,1)S(1)} collective-permute-done((bf16[80,2048]{1,0:T(8,128)(2,1)S(1)}, bf16[80,2048]{1,0:T(8,128)(2,1)S(1)}, u32[]{:S(2)}, u32[]{:S(2)}) %collective-permute-start.10) | collective-permute-done | bytes 327712 | tf_op jit(solution)/shard_map/ppermute | solution.py:98
  42.5 0.0 collective-permute-start.7
  42.5 0.0 collective-permute-done.26.refs_2_
  42.5 0.5 collective-permute-start.19
  43.0 3.1 %collective-permute-done.18.refs_1_ = bf16[80,2048]{1,0:T(8,128)(2,1)S(1)} collective-permute-done((bf16[80,2048]{1,0:T(8,128)(2,1)S(1)}, bf16[80,2048]{1,0:T(8,128)(2,1)S(1)}, u32[]{:S(2)}, u32[]{:S(2)}) %collective-permute-start.18) | collective-permute-done | bytes 327712 | tf_op jit(solution)/shard_map/ppermute | solution.py:98
  46.2 1.5 %collective-permute-start.11 = (bf16[80,2048]{1,0:T(8,128)(2,1)S(1)}, bf16[80,2048]{1,0:T(8,128)(2,1)S(1)}, u32[]{:S(2)}, u32[]{:S(2)}) collective-permute-start(bf16[80,2048]{1,0:T(8,128)(2,1)S(1)} %collective-permute-done.10.refs_0_), channel_id=1, source_target_pairs={{0,2},{1,3},{2,0},{3,1},{4,6},{5,7},{6,4},{7,5},{8,10},{9,11},{10,... | collective-permute-start | bytes 983048 | tf_op jit(solution)/shard_map/ppermute | solution.py:98
  47.7 6.6 %shard_map.163 = (bf16[80,2048]{1,0:T(8,128)(2,1)S(1)}, bf16[80,2048]{1,0:T(8,128)(2,1)S(1)}, bf16[160,2048]{1,0:T(8,128)(2,1)S(1)}) custom-call(bf16[80,2048]{1,0:T(8,128)(2,1)S(1)} %collective-permute-done.24.refs_0_, bf16[80,2048]{1,0:T(8,128)(2,1)S(1)} %collective-permute-done.25.refs_1_, bf16[80,2048]{1,0:T(8,128)(2,1)S(1)} %collective-permute-done.26.refs_2_, ...), custom_call_target="tpu_custom_call" | custom-call | flops 3523215360 | bytes 11010048 | tf_op jit(solution)/shard_map/pallas_call | solution.py:501
  54.3 0.6 collective-permute-start.12
  54.9 0.1 collective-permute-start.8
  55.0 3.4 %collective-permute-done.11.refs_1_ = bf16[80,2048]{1,0:T(8,128)(2,1)S(1)} collective-permute-done((bf16[80,2048]{1,0:T(8,128)(2,1)S(1)}, bf16[80,2048]{1,0:T(8,128)(2,1)S(1)}, u32[]{:S(2)}, u32[]{:S(2)}) %collective-permute-start.11) | collective-permute-done | bytes 327712 | tf_op jit(solution)/shard_map/ppermute | solution.py:98
  58.4 0.5 collective-permute-start.28
  58.9 6.6 %shard_map.160 = (bf16[80,2048]{1,0:T(8,128)(2,1)S(1)}, bf16[80,2048]{1,0:T(8,128)(2,1)S(1)}, bf16[160,2048]{1,0:T(8,128)(2,1)S(1)}) custom-call(bf16[80,2048]{1,0:T(8,128)(2,1)S(1)} %collective-permute-done.17.refs_0_, bf16[80,2048]{1,0:T(8,128)(2,1)S(1)} %collective-permute-done.18.refs_1_, bf16[80,2048]{1,0:T(8,128)(2,1)S(1)} %collective-permute-done.19.refs_2_, ...), custom_call_target="tpu_custom_call" | custom-call | flops 3523215360 | bytes 11010048 | tf_op jit(solution)/shard_map/pallas_call | solution.py:501
  65.5 0.1 collective-permute-start.21
  65.6 6.6 %shard_map.157 = (bf16[80,2048]{1,0:T(8,128)(2,1)S(1)}, bf16[80,2048]{1,0:T(8,128)(2,1)S(1)}, bf16[160,2048]{1,0:T(8,128)(2,1)S(1)}) custom-call(bf16[80,2048]{1,0:T(8,128)(2,1)S(1)} %collective-permute-done.10.refs_0_, bf16[80,2048]{1,0:T(8,128)(2,1)S(1)} %collective-permute-done.11.refs_1_, bf16[80,2048]{1,0:T(8,128)(2,1)S(1)} %collective-permute-done.12.refs_2_, ...), custom_call_target="tpu_custom_call" | custom-call | flops 3523215360 | bytes 11010048 | tf_op jit(solution)/shard_map/pallas_call | solution.py:501
  72.3 0.6 collective-permute-start.14
  72.8 6.8 %shard_map.155 = (bf16[80,2048]{1,0:T(8,128)(2,1)S(1)}, bf16[80,2048]{1,0:T(8,128)(2,1)S(1)}, bf16[160,2048]{1,0:T(8,128)(2,1)S(1)}) custom-call(bf16[80,2048]{1,0:T(8,128)(2,1)S(1)} %get-tuple-element.36.refs_0_, bf16[80,2048]{1,0:T(8,128)(2,1)S(1)} %collective-permute-done.6.refs_1_, bf16[80,2048]{1,0:T(8,128)(2,1)S(1)} %collective-permute-done.7.refs_2_, ...), custom_call_target="tpu_custom_call" | custom-call | flops 3523215360 | bytes 11010048 | tf_op jit(solution)/shard_map/pallas_call | solution.py:501
  79.7 0.0 copy-start.1
  79.7 0.0 copy-start.2
  79.7 0.0 copy-start.3
  79.7 0.0 copy-start.6
  79.7 0.0 copy-start.7
  79.7 0.0 copy-start.8
  79.7 0.1 collective-permute-start.9
  79.8 0.2 shard_map.164
  80.0 1.6 %collective-permute-start.29 = (bf16[80,2048]{1,0:T(8,128)(2,1)S(1)}, bf16[80,2048]{1,0:T(8,128)(2,1)S(1)}, u32[]{:S(2)}, u32[]{:S(2)}) collective-permute-start(bf16[80,2048]{1,0:T(8,128)(2,1)S(1)} %get-tuple-element.58), channel_id=1, source_target_pairs={{0,2},{1,3},{2,0},{3,1},{4,6},{5,7},{6,4},{7,5},{8,10},{9,11},{10,... | collective-permute-start | bytes 983048 | tf_op jit(solution)/shard_map/ppermute | solution.py:98
  81.6 0.2 shard_map.161
  81.7 0.6 collective-permute-start.22
  82.3 0.2 shard_map.158
  82.5 1.6 %collective-permute-start.15 = (bf16[80,2048]{1,0:T(8,128)(2,1)S(1)}, bf16[80,2048]{1,0:T(8,128)(2,1)S(1)}, u32[]{:S(2)}, u32[]{:S(2)}) collective-permute-start(bf16[80,2048]{1,0:T(8,128)(2,1)S(1)} %get-tuple-element.46), channel_id=1, source_target_pairs={{0,2},{1,3},{2,0},{3,1},{4,6},{5,7},{6,4},{7,5},{8,10},{9,11},{10,... | collective-permute-start | bytes 983048 | tf_op jit(solution)/shard_map/ppermute | solution.py:98
  84.1 0.9 shard_map.149
  85.0 2.4 %collective-permute-start = (f32[2,136,128]{2,1,0:T(8,128)S(1)}, f32[2,136,128]{2,1,0:T(8,128)S(1)}, u32[]{:S(2)}, u32[]{:S(2)}) collective-permute-start(f32[2,136,128]{2,1,0:T(8,128)S(1)} %get-tuple-element.33), channel_id=1, source_target_pairs={{0,4},{1,5},{2,6},{3,7},{16,20},{17,21},{18,22},{19,23}} | collective-permute-start | bytes 417800 | tf_op jit(solution)/shard_map/ppermute | solution.py:322
  87.4 2.7 %collective-permute-done.refs_0_ = f32[2,136,128]{2,1,0:T(8,128)S(1)} collective-permute-done((f32[2,136,128]{2,1,0:T(8,128)S(1)}, f32[2,136,128]{2,1,0:T(8,128)S(1)}, u32[]{:S(2)}, u32[]{:S(2)}) %collective-permute-start) | collective-permute-done | bytes 139296 | tf_op jit(solution)/shard_map/ppermute | solution.py:322
  90.2 0.7 collective-permute-start.1
  90.9 0.7 collective-permute-start.2
  91.6 0.8 shard_map.156
  92.4 0.5 collective-permute-start.31
  92.9 0.1 shard_map.165
  93.0 0.1 collective-permute-start.30
  93.1 4.6 %collective-permute-done.22.other = bf16[80,2048]{1,0:T(8,128)(2,1)S(1)} collective-permute-done((bf16[80,2048]{1,0:T(8,128)(2,1)S(1)}, bf16[80,2048]{1,0:T(8,128)(2,1)S(1)}, u32[]{:S(2)}, u32[]{:S(2)}) %collective-permute-start.22) | collective-permute-done | bytes 327712 | tf_op jit(solution)/shard_map/ppermute | solution.py:98
  97.7 0.1 shard_map.162
  97.7 10.5 %collective-permute-start.23 = (bf16[80,2048]{1,0:T(8,128)(2,1)S(1)}, bf16[80,2048]{1,0:T(8,128)(2,1)S(1)}, u32[]{:S(2)}, u32[]{:S(2)}) collective-permute-start(bf16[80,2048]{1,0:T(8,128)(2,1)S(1)} %shard_map.162), channel_id=1, source_target_pairs={{0,8},{4,12},{8,0},{12,4},{1,9},{5,13},{9,1},{13,5},{2,10},{6,14},... | collective-permute-start | bytes 983048 | tf_op jit(solution)/shard_map/ppermute | solution.py:98
  108.2 0.8 shard_map.159
  109.0 0.6 collective-permute-start.16
  109.6 0.8 shard_map.152.own
  110.4 1.4 %collective-permute-start.3 = (bf16[128,256]{1,0:T(8,128)(2,1)S(1)}, bf16[128,256]{1,0:T(8,128)(2,1)S(1)}, u32[]{:S(2)}, u32[]{:S(2)}) collective-permute-start(bf16[128,256]{1,0:T(8,128)(2,1)S(1)} %shard_map.152.own), channel_id=1, source_target_pairs={{0,2},{1,3},{2,0},{3,1},{4,6},{5,7},{6,4},{7,5},{8,10},{9,11},{10,... | collective-permute-start | bytes 196616 | tf_op jit(solution)/shard_map/ppermute | solution.py:98
  111.8 2.9 %collective-permute-done.3.across = bf16[128,256]{1,0:T(8,128)(2,1)S(1)} collective-permute-done((bf16[128,256]{1,0:T(8,128)(2,1)S(1)}, bf16[128,256]{1,0:T(8,128)(2,1)S(1)}, u32[]{:S(2)}, u32[]{:S(2)}) %collective-permute-start.3) | collective-permute-done | bytes 65568 | tf_op jit(solution)/shard_map/ppermute | solution.py:98
  114.7 1.3 collective-permute-done.4.beside
  115.9 0.6 copy-done.4
  116.6 0.2 collective-permute-start.5
  116.7 1.2 collective-permute-done.5.corner
  118.0 0.8 copy-done.5
  118.8 1.8 %shard_map.153 = bf16[128,512]{1,0:T(8,128)(2,1)} custom-call(s32[1]{0:T(128)} %bitcast.place, bf16[128,256]{1,0:T(8,128)(2,1)S(1)} %shard_map.152.own, bf16[128,256]{1,0:T(8,128)(2,1)S(1)} %collective-permute-done.3.across, bf16[128,256]{1,0:T(8,128)(2,1)S(1)} %copy-done.5, bf16[128,256]{1,0:T(8,128)(2,1)} %collective-permute-done.5.corner, ...), custom_call_target="tpu_custom_call" | custom-call | tf_op jit(solution)/shard_map/pallas_call | solution.py:334
  120.6 8.0 %collective-permute-done.23.refs_3_ = bf16[80,2048]{1,0:T(8,128)(2,1)S(1)} collective-permute-done((bf16[80,2048]{1,0:T(8,128)(2,1)S(1)}, bf16[80,2048]{1,0:T(8,128)(2,1)S(1)}, u32[]{:S(2)}, u32[]{:S(2)}) %collective-permute-start.23) | collective-permute-done | bytes 327712 | tf_op jit(solution)/shard_map/ppermute | solution.py:98
  128.6 1.7 %shard_map.166 = bf16[128,2048]{1,0:T(8,128)(2,1)} custom-call(f32[128,128]{1,0:T(8,128)S(1)} %get-tuple-element.35.refs_0_, bf16[80,2048]{1,0:T(8,128)(2,1)S(1)} %get-tuple-element.40.refs_1_, bf16[80,2048]{1,0:T(8,128)(2,1)S(1)} %collective-permute-done.16.refs_2_, bf16[80,2048]{1,0:T(8,128)(2,1)S(1)} %collective-permute-done.23.refs_3_, ...), custom_call_target="tpu_custom_call" | custom-call | tf_op jit(solution)/shard_map/pallas_call | solution.py:457
  (36 shorter events, 0.2 us)
Async XLA Ops:
  2.4 13.8 %collective-permute-start.24 = (bf16[80,2048]{1,0:T(8,128)(2,1)S(1)}, bf16[80,2048]{1,0:T(8,128)(2,1)S(1)}, u32[]{:S(2)}, u32[]{:S(2)}) collective-permute-start(bf16[80,2048]{1,0:T(8,128)(2,1)S(1)} %get-tuple-element.53), channel_id=1, source_target_pairs={{0,12},{4,8},{8,4},{12,0},{1,13},{5,9},{9,5},{13,1},{2,14},{6,10},... | collective-permute-start | bytes 983048 | tf_op jit(solution)/shard_map/ppermute | solution.py:98
  7.6 28.0 %collective-permute-start.17 = (bf16[80,2048]{1,0:T(8,128)(2,1)S(1)}, bf16[80,2048]{1,0:T(8,128)(2,1)S(1)}, u32[]{:S(2)}, u32[]{:S(2)}) collective-permute-start(bf16[80,2048]{1,0:T(8,128)(2,1)S(1)} %get-tuple-element.47), channel_id=1, source_target_pairs={{0,8},{4,12},{8,0},{12,4},{1,9},{5,13},{9,1},{13,5},{2,10},{6,14},... | collective-permute-start | bytes 983048 | tf_op jit(solution)/shard_map/ppermute | solution.py:98
  16.2 20.9 %collective-permute-start.25 = (bf16[80,2048]{1,0:T(8,128)(2,1)S(1)}, bf16[80,2048]{1,0:T(8,128)(2,1)S(1)}, u32[]{:S(2)}, u32[]{:S(2)}) collective-permute-start(bf16[80,2048]{1,0:T(8,128)(2,1)S(1)} %collective-permute-done.24.refs_0_), channel_id=1, source_target_pairs={{0,2},{1,3},{2,0},{3,1},{4,6},{5,7},{6,4},{7,5},{8,10},{9,11},{10,... | collective-permute-start | bytes 983048 | tf_op jit(solution)/shard_map/ppermute | solution.py:98
  17.9 24.6 %collective-permute-start.10 = (bf16[80,2048]{1,0:T(8,128)(2,1)S(1)}, bf16[80,2048]{1,0:T(8,128)(2,1)S(1)}, u32[]{:S(2)}, u32[]{:S(2)}) collective-permute-start(bf16[80,2048]{1,0:T(8,128)(2,1)S(1)} %get-tuple-element.41), channel_id=1, source_target_pairs={{0,4},{4,0},{8,12},{12,8},{1,5},{5,1},{9,13},{13,9},{2,6},{6,2},{1... | collective-permute-start | bytes 983048 | tf_op jit(solution)/shard_map/ppermute | solution.py:98
  31.5 11.1 %collective-permute-start.26 = (bf16[80,2048]{1,0:T(8,128)(2,1)S(1)}, bf16[80,2048]{1,0:T(8,128)(2,1)S(1)}, u32[]{:S(2)}, u32[]{:S(2)}) collective-permute-start(bf16[80,2048]{1,0:T(8,128)(2,1)S(1)} %collective-permute-done.24.refs_0_), channel_id=1, source_target_pairs={{0,1},{1,0},{2,3},{3,2},{4,5},{5,4},{6,7},{7,6},{8,9},{9,8},{10,11... | collective-permute-start | bytes 983048 | tf_op jit(solution)/shard_map/ppermute | solution.py:98
  35.6 10.6 %collective-permute-start.18 = (bf16[80,2048]{1,0:T(8,128)(2,1)S(1)}, bf16[80,2048]{1,0:T(8,128)(2,1)S(1)}, u32[]{:S(2)}, u32[]{:S(2)}) collective-permute-start(bf16[80,2048]{1,0:T(8,128)(2,1)S(1)} %collective-permute-done.17.refs_0_), channel_id=1, source_target_pairs={{0,2},{1,3},{2,0},{3,1},{4,6},{5,7},{6,4},{7,5},{8,10},{9,11},{10,... | collective-permute-start | bytes 983048 | tf_op jit(solution)/shard_map/ppermute | solution.py:98
  37.1 10.6 %collective-permute-start.27 = (bf16[80,2048]{1,0:T(8,128)(2,1)S(1)}, bf16[80,2048]{1,0:T(8,128)(2,1)S(1)}, u32[]{:S(2)}, u32[]{:S(2)}) collective-permute-start(bf16[80,2048]{1,0:T(8,128)(2,1)S(1)} %collective-permute-done.25.refs_1_), channel_id=1, source_target_pairs={{0,1},{1,0},{2,3},{3,2},{4,5},{5,4},{6,7},{7,6},{8,9},{9,8},{10,11... | collective-permute-start | bytes 983048 | tf_op jit(solution)/shard_map/ppermute | solution.py:98
  37.1 17.2 %collective-permute-start.6 = (bf16[80,2048]{1,0:T(8,128)(2,1)S(1)}, bf16[80,2048]{1,0:T(8,128)(2,1)S(1)}, u32[]{:S(2)}, u32[]{:S(2)}) collective-permute-start(bf16[80,2048]{1,0:T(8,128)(2,1)S(1)} %get-tuple-element.36.refs_0_), channel_id=1, source_target_pairs={{0,2},{1,3},{2,0},{3,1},{4,6},{5,7},{6,4},{7,5},{8,10},{9,11},{10,... | collective-permute-start | bytes 983048 | tf_op jit(solution)/shard_map/ppermute | solution.py:98
  42.5 30.3 %collective-permute-start.7 = (bf16[80,2048]{1,0:T(8,128)(2,1)S(1)}, bf16[80,2048]{1,0:T(8,128)(2,1)S(1)}, u32[]{:S(2)}, u32[]{:S(2)}) collective-permute-start(bf16[80,2048]{1,0:T(8,128)(2,1)S(1)} %get-tuple-element.36.refs_0_), channel_id=1, source_target_pairs={{0,1},{1,0},{2,3},{3,2},{4,5},{5,4},{6,7},{7,6},{8,9},{9,8},{10,11... | collective-permute-start | bytes 983048 | tf_op jit(solution)/shard_map/ppermute | solution.py:98
  42.5 12.4 %collective-permute-start.19 = (bf16[80,2048]{1,0:T(8,128)(2,1)S(1)}, bf16[80,2048]{1,0:T(8,128)(2,1)S(1)}, u32[]{:S(2)}, u32[]{:S(2)}) collective-permute-start(bf16[80,2048]{1,0:T(8,128)(2,1)S(1)} %collective-permute-done.17.refs_0_), channel_id=1, source_target_pairs={{0,1},{1,0},{2,3},{3,2},{4,5},{5,4},{6,7},{7,6},{8,9},{9,8},{10,11... | collective-permute-start | bytes 983048 | tf_op jit(solution)/shard_map/ppermute | solution.py:98
  46.2 12.2 %collective-permute-start.11 = (bf16[80,2048]{1,0:T(8,128)(2,1)S(1)}, bf16[80,2048]{1,0:T(8,128)(2,1)S(1)}, u32[]{:S(2)}, u32[]{:S(2)}) collective-permute-start(bf16[80,2048]{1,0:T(8,128)(2,1)S(1)} %collective-permute-done.10.refs_0_), channel_id=1, source_target_pairs={{0,2},{1,3},{2,0},{3,1},{4,6},{5,7},{6,4},{7,5},{8,10},{9,11},{10,... | collective-permute-start | bytes 983048 | tf_op jit(solution)/shard_map/ppermute | solution.py:98
  47.7 10.7 %collective-permute-start.20 = (bf16[80,2048]{1,0:T(8,128)(2,1)S(1)}, bf16[80,2048]{1,0:T(8,128)(2,1)S(1)}, u32[]{:S(2)}, u32[]{:S(2)}) collective-permute-start(bf16[80,2048]{1,0:T(8,128)(2,1)S(1)} %collective-permute-done.18.refs_1_), channel_id=1, source_target_pairs={{0,1},{1,0},{2,3},{3,2},{4,5},{5,4},{6,7},{7,6},{8,9},{9,8},{10,11... | collective-permute-start | bytes 983048 | tf_op jit(solution)/shard_map/ppermute | solution.py:98
  54.3 11.2 %collective-permute-start.12 = (bf16[80,2048]{1,0:T(8,128)(2,1)S(1)}, bf16[80,2048]{1,0:T(8,128)(2,1)S(1)}, u32[]{:S(2)}, u32[]{:S(2)}) collective-permute-start(bf16[80,2048]{1,0:T(8,128)(2,1)S(1)} %collective-permute-done.10.refs_0_), channel_id=1, source_target_pairs={{0,1},{1,0},{2,3},{3,2},{4,5},{5,4},{6,7},{7,6},{8,9},{9,8},{10,11... | collective-permute-start | bytes 983048 | tf_op jit(solution)/shard_map/ppermute | solution.py:98
  54.9 17.9 %collective-permute-start.8 = (bf16[80,2048]{1,0:T(8,128)(2,1)S(1)}, bf16[80,2048]{1,0:T(8,128)(2,1)S(1)}, u32[]{:S(2)}, u32[]{:S(2)}) collective-permute-start(bf16[80,2048]{1,0:T(8,128)(2,1)S(1)} %collective-permute-done.6.refs_1_), channel_id=1, source_target_pairs={{0,1},{1,0},{2,3},{3,2},{4,5},{5,4},{6,7},{7,6},{8,9},{9,8},{10,11... | collective-permute-start | bytes 983048 | tf_op jit(solution)/shard_map/ppermute | solution.py:98
  58.4 7.2 %collective-permute-start.13 = (bf16[80,2048]{1,0:T(8,128)(2,1)S(1)}, bf16[80,2048]{1,0:T(8,128)(2,1)S(1)}, u32[]{:S(2)}, u32[]{:S(2)}) collective-permute-start(bf16[80,2048]{1,0:T(8,128)(2,1)S(1)} %collective-permute-done.11.refs_1_), channel_id=1, source_target_pairs={{0,1},{1,0},{2,3},{3,2},{4,5},{5,4},{6,7},{7,6},{8,9},{9,8},{10,11... | collective-permute-start | bytes 983048 | tf_op jit(solution)/shard_map/ppermute | solution.py:98
  58.4 21.5 %collective-permute-start.28 = (bf16[160,2048]{1,0:T(8,128)(2,1)S(1)}, bf16[160,2048]{1,0:T(8,128)(2,1)S(1)}, u32[]{:S(2)}, u32[]{:S(2)}) collective-permute-start(bf16[160,2048]{1,0:T(8,128)(2,1)S(1)} %get-tuple-element.56), channel_id=1, source_target_pairs={{0,1},{1,0},{2,3},{3,2},{4,5},{5,4},{6,7},{7,6},{8,9},{9,8},{10,11... | collective-permute-start | bytes 1966088 | tf_op jit(solution)/shard_map/ppermute | solution.py:98
  65.5 16.0 %collective-permute-start.21 = (bf16[160,2048]{1,0:T(8,128)(2,1)S(1)}, bf16[160,2048]{1,0:T(8,128)(2,1)S(1)}, u32[]{:S(2)}, u32[]{:S(2)}) collective-permute-start(bf16[160,2048]{1,0:T(8,128)(2,1)S(1)} %get-tuple-element.50), channel_id=1, source_target_pairs={{0,1},{1,0},{2,3},{3,2},{4,5},{5,4},{6,7},{7,6},{8,9},{9,8},{10,11... | collective-permute-start | bytes 1966088 | tf_op jit(solution)/shard_map/ppermute | solution.py:98
  72.3 10.0 %collective-permute-start.14 = (bf16[160,2048]{1,0:T(8,128)(2,1)S(1)}, bf16[160,2048]{1,0:T(8,128)(2,1)S(1)}, u32[]{:S(2)}, u32[]{:S(2)}) collective-permute-start(bf16[160,2048]{1,0:T(8,128)(2,1)S(1)} %get-tuple-element.44), channel_id=1, source_target_pairs={{0,1},{1,0},{2,3},{3,2},{4,5},{5,4},{6,7},{7,6},{8,9},{9,8},{10,11... | collective-permute-start | bytes 1966088 | tf_op jit(solution)/shard_map/ppermute | solution.py:98
  79.7 4.4 %copy-start.1 = (bf16[128,256]{1,0:T(8,128)(2,1)S(1)}, bf16[128,256]{1,0:T(8,128)(2,1)}, u32[]{:S(2)}) copy-start(bf16[128,256]{1,0:T(8,128)(2,1)} %query.3) | copy-start | bytes 196612
  79.7 4.4 %copy-start.2 = (bf16[128,256]{1,0:T(8,128)(2,1)S(1)}, bf16[128,256]{1,0:T(8,128)(2,1)}, u32[]{:S(2)}) copy-start(bf16[128,256]{1,0:T(8,128)(2,1)} %key.1) | copy-start | bytes 196612
  79.7 4.4 %copy-start.3 = (bf16[128,256]{1,0:T(8,128)(2,1)S(1)}, bf16[128,256]{1,0:T(8,128)(2,1)}, u32[]{:S(2)}) copy-start(bf16[128,256]{1,0:T(8,128)(2,1)} %value.1) | copy-start | bytes 196612
  79.7 4.3 %copy-start.6 = (f32[2,128]{1,0:T(2,128)S(1)}, f32[2,128]{1,0:T(2,128)}, u32[]{:S(2)}) copy-start(f32[2,128]{1,0:T(2,128)} %gate.1) | copy-start | bytes 3076
  79.7 4.3 %copy-start.7 = (f32[2,128]{1,0:T(2,128)S(1)}, f32[2,128]{1,0:T(2,128)}, u32[]{:S(2)}) copy-start(f32[2,128]{1,0:T(2,128)} %logits.1) | copy-start | bytes 3076
  79.7 4.3 %copy-start.8 = (f32[2,128]{1,0:T(2,128)S(1)}, f32[2,128]{1,0:T(2,128)}, u32[]{:S(2)}) copy-start(f32[2,128]{1,0:T(2,128)} %extra.1) | copy-start | bytes 3076
  79.7 11.9 %collective-permute-start.9 = (bf16[160,2048]{1,0:T(8,128)(2,1)S(1)}, bf16[160,2048]{1,0:T(8,128)(2,1)S(1)}, u32[]{:S(2)}, u32[]{:S(2)}) collective-permute-start(bf16[160,2048]{1,0:T(8,128)(2,1)S(1)} %get-tuple-element.39), channel_id=1, source_target_pairs={{0,1},{1,0},{2,3},{3,2},{4,5},{5,4},{6,7},{7,6},{8,9},{9,8},{10,11... | collective-permute-start | bytes 1966088 | tf_op jit(solution)/shard_map/ppermute | solution.py:98
  80.0 12.9 %collective-permute-start.29 = (bf16[80,2048]{1,0:T(8,128)(2,1)S(1)}, bf16[80,2048]{1,0:T(8,128)(2,1)S(1)}, u32[]{:S(2)}, u32[]{:S(2)}) collective-permute-start(bf16[80,2048]{1,0:T(8,128)(2,1)S(1)} %get-tuple-element.58), channel_id=1, source_target_pairs={{0,2},{1,3},{2,0},{3,1},{4,6},{5,7},{6,4},{7,5},{8,10},{9,11},{10,... | collective-permute-start | bytes 983048 | tf_op jit(solution)/shard_map/ppermute | solution.py:98
  81.7 15.9 %collective-permute-start.22 = (bf16[80,2048]{1,0:T(8,128)(2,1)S(1)}, bf16[80,2048]{1,0:T(8,128)(2,1)S(1)}, u32[]{:S(2)}, u32[]{:S(2)}) collective-permute-start(bf16[80,2048]{1,0:T(8,128)(2,1)S(1)} %get-tuple-element.52), channel_id=1, source_target_pairs={{0,2},{1,3},{2,0},{3,1},{4,6},{5,7},{6,4},{7,5},{8,10},{9,11},{10,... | collective-permute-start | bytes 983048 | tf_op jit(solution)/shard_map/ppermute | solution.py:98
  82.3 35.7 %copy-start = (bf16[1024,512]{1,0:T(8,128)(2,1)S(1)}, bf16[1024,512]{1,0:T(8,128)(2,1)}, u32[]{:S(2)}) copy-start(bf16[1024,512]{1,0:T(8,128)(2,1)} %weight.1) | copy-start | bytes 3145732
  82.5 25.7 %collective-permute-start.15 = (bf16[80,2048]{1,0:T(8,128)(2,1)S(1)}, bf16[80,2048]{1,0:T(8,128)(2,1)S(1)}, u32[]{:S(2)}, u32[]{:S(2)}) collective-permute-start(bf16[80,2048]{1,0:T(8,128)(2,1)S(1)} %get-tuple-element.46), channel_id=1, source_target_pairs={{0,2},{1,3},{2,0},{3,1},{4,6},{5,7},{6,4},{7,5},{8,10},{9,11},{10,... | collective-permute-start | bytes 983048 | tf_op jit(solution)/shard_map/ppermute | solution.py:98
  85.0 5.1 %collective-permute-start = (f32[2,136,128]{2,1,0:T(8,128)S(1)}, f32[2,136,128]{2,1,0:T(8,128)S(1)}, u32[]{:S(2)}, u32[]{:S(2)}) collective-permute-start(f32[2,136,128]{2,1,0:T(8,128)S(1)} %get-tuple-element.33), channel_id=1, source_target_pairs={{0,4},{1,5},{2,6},{3,7},{16,20},{17,21},{18,22},{19,23}} | collective-permute-start | bytes 417800 | tf_op jit(solution)/shard_map/ppermute | solution.py:322
  90.2 0.7 collective-permute-start.1
  90.9 18.7 %collective-permute-start.2 = (f32[2,136,128]{2,1,0:T(8,128)S(1)}, f32[2,136,128]{2,1,0:T(8,128)S(1)}, u32[]{:S(2)}, u32[]{:S(2)}) collective-permute-start(f32[2,136,128]{2,1,0:T(8,128)S(1)} %shard_map.151), channel_id=1, source_target_pairs={{8,12},{9,13},{10,14},{11,15},{24,28},{25,29},{26,30},{27,31}} | collective-permute-start | bytes 417800 | tf_op jit(solution)/shard_map/ppermute | solution.py:322
  92.4 28.2 %collective-permute-start.31 = (bf16[80,2048]{1,0:T(8,128)(2,1)}, bf16[80,2048]{1,0:T(8,128)(2,1)S(1)}, u32[]{:S(2)}, u32[]{:S(2)}) collective-permute-start(bf16[80,2048]{1,0:T(8,128)(2,1)} %get-tuple-element.59), channel_id=1, source_target_pairs={{0,2},{1,3},{2,0},{3,1},{4,6},{5,7},{6,4},{7,5},{8,10},{9,11},{10,... | collective-permute-start | bytes 983048 | tf_op jit(solution)/shard_map/ppermute | solution.py:98
  93.0 27.6 %collective-permute-start.30 = (bf16[80,2048]{1,0:T(8,128)(2,1)S(1)}, bf16[80,2048]{1,0:T(8,128)(2,1)S(1)}, u32[]{:S(2)}, u32[]{:S(2)}) collective-permute-start(bf16[80,2048]{1,0:T(8,128)(2,1)S(1)} %shard_map.165), channel_id=1, source_target_pairs={{0,12},{4,8},{8,4},{12,0},{1,13},{5,9},{9,5},{13,1},{2,14},{6,10},... | collective-permute-start | bytes 983048 | tf_op jit(solution)/shard_map/ppermute | solution.py:98
  97.7 30.9 %collective-permute-start.23 = (bf16[80,2048]{1,0:T(8,128)(2,1)S(1)}, bf16[80,2048]{1,0:T(8,128)(2,1)S(1)}, u32[]{:S(2)}, u32[]{:S(2)}) collective-permute-start(bf16[80,2048]{1,0:T(8,128)(2,1)S(1)} %shard_map.162), channel_id=1, source_target_pairs={{0,8},{4,12},{8,0},{12,4},{1,9},{5,13},{9,1},{13,5},{2,10},{6,14},... | collective-permute-start | bytes 983048 | tf_op jit(solution)/shard_map/ppermute | solution.py:98
  109.0 19.6 %collective-permute-start.16 = (bf16[80,2048]{1,0:T(8,128)(2,1)}, bf16[80,2048]{1,0:T(8,128)(2,1)S(1)}, u32[]{:S(2)}, u32[]{:S(2)}) collective-permute-start(bf16[80,2048]{1,0:T(8,128)(2,1)} %shard_map.159), channel_id=1, source_target_pairs={{0,4},{4,0},{8,12},{12,8},{1,5},{5,1},{9,13},{13,9},{2,6},{6,2},{1... | collective-permute-start | bytes 983048 | tf_op jit(solution)/shard_map/ppermute | solution.py:98
  110.4 4.3 %collective-permute-start.3 = (bf16[128,256]{1,0:T(8,128)(2,1)S(1)}, bf16[128,256]{1,0:T(8,128)(2,1)S(1)}, u32[]{:S(2)}, u32[]{:S(2)}) collective-permute-start(bf16[128,256]{1,0:T(8,128)(2,1)S(1)} %shard_map.152.own), channel_id=1, source_target_pairs={{0,2},{1,3},{2,0},{3,1},{4,6},{5,7},{6,4},{7,5},{8,10},{9,11},{10,... | collective-permute-start | bytes 196616 | tf_op jit(solution)/shard_map/ppermute | solution.py:98
  114.7 1.3 collective-permute-start.4
  115.9 0.6 copy-start.4
  116.6 1.4 %collective-permute-start.5 = (bf16[128,256]{1,0:T(8,128)(2,1)S(1)}, bf16[128,256]{1,0:T(8,128)(2,1)}, u32[]{:S(2)}, u32[]{:S(2)}) collective-permute-start(bf16[128,256]{1,0:T(8,128)(2,1)S(1)} %collective-permute-done.3.across), channel_id=1, source_target_pairs={{0,1},{1,0},{2,3},{3,2},{4,5},{5,4},{6,7},{7,6},{8,9},{9,8},{10,11... | collective-permute-start | bytes 196616 | tf_op jit(solution)/shard_map/ppermute | solution.py:98
  118.0 0.8 copy-start.5
where the time goes:
time: 131 us; the launch traced here: 130 us
  starting transfers between devices  47 us (36%)
  waiting for transfers between devices  44.9 us (34%)
  Pallas kernels  36 us (27%)
  local copies, waits for them, and re-layouts  1.51 us (1%)
    ppermute x29, starting transfers between devices, swap(): return lax.ppermute(rows, axis, [(i, i ^ bit) for i in range(size)])  43.2 us
    ppermute x29, waiting for transfers between devices, swap(): return lax.ppermute(rows, axis, [(i, i ^ bit) for i in range(size)])  42.2 us
    pallas_call x4, Pallas kernels, expert_rows(): pl.pallas_call(expert_kernel, in_specs=[vmem] * 4 + [hbm] * 3, out_specs=...  26.7 us
    ppermute x3, starting transfers between devices, memory_pairs(): earlier.append(lax.ppermute(after, 'ep', [(hop, hop + 1)]))  3.78 us
    ppermute x3, waiting for transfers between devices, memory_pairs(): earlier.append(lax.ppermute(after, 'ep', [(hop, hop + 1)]))  2.71 us
  transfers between devices with their start and end apart: 32, of which 11 were waited for; matrix products, arithmetic and copies ran while one was open for 0% of the time, Pallas kernels for 25%

commit v1 on v0

--- a/solution.py
+++ b/solution.py
@@ -179,7 +179,18 @@
     return both[: left.shape[0]] + both[left.shape[0] :]
 
 
-def local_kernel(query, key, value, gate, logits, extra, local, after, inside, columns):
+def local_kernel(*refs):
+    sources = refs[:6]
+    local, after, inside, columns = refs[6:10]
+    query, key, value, gate, logits, extra, sems = refs[10:]
+    copies = [
+        pltpu.make_async_copy(source, target, sems.at[n])
+        for n, (source, target) in enumerate(zip(sources, refs[10:16], strict=True))
+    ]
+    for copy in copies:
+        copy.start()
+    for copy in copies:
+        copy.wait()
     heads = gate.shape[0]
     size = query.shape[0]
     scale = DH ** (-0.5)
@@ -291,7 +302,7 @@
     packed = jax.ShapeDtypeStruct((heads, DH + 8, DH), jnp.float32)
     local, after, inside, columns = pl.pallas_call(
         local_kernel,
-        in_specs=[vmem] * 6,
+        in_specs=[pl.BlockSpec(memory_space=pltpu.HBM)] * 6,
         out_specs=[vmem] * 4,
         out_shape=[
             packed,
@@ -299,14 +310,17 @@
             jax.ShapeDtypeStruct((size, width), jnp.float32),
             jax.ShapeDtypeStruct((size, size), jnp.float32),
         ],
+        scratch_shapes=[pltpu.VMEM((size, width), jnp.bfloat16)] * 3
+        + [pltpu.VMEM((heads, size), jnp.float32)] * 3
+        + [pltpu.SemaphoreType.DMA((6,))],
         compiler_params=params,
     )(
-        memory_query_rows,
-        memory_key_rows,
-        memory_value_rows,
-        input_gate_log,
-        forget_gate_logits,
-        forget_log_extra,
+        in_hbm(memory_query_rows),
+        in_hbm(memory_key_rows),
+        in_hbm(memory_value_rows),
+        in_hbm(input_gate_log),
+        in_hbm(forget_gate_logits),
+        in_hbm(forget_log_extra),
     )
     earlier = []
     hops = lax.axis_size("ep") - 1
@@ -464,62 +478,65 @@
     )(table, *returned)
 
 
-def expert_kernel(*refs):
-    pieces = refs[:4]
-    gate, up, down = refs[4:7]
-    outs = refs[7:10]
-    rows, hidden, gate_here, up_here, down_here, sems = refs[10:]
+def load_kernel(gate, up, down, gate_here, up_here, down_here, sems):
     copies = [
-        pltpu.make_async_copy(gate.at[0], gate_here, sems.at[0]),
-        pltpu.make_async_copy(up.at[0], up_here, sems.at[1]),
-        pltpu.make_async_copy(down.at[0], down_here, sems.at[2]),
+        pltpu.make_async_copy(source.at[0], target, sems.at[n])
+        for n, (source, target) in enumerate(
+            ((gate, gate_here), (up, up_here), (down, down_here))
+        )
     ]
     for copy in copies:
         copy.start()
-    at = 0
-    for piece in pieces:
-        rows[at : at + piece.shape[0], :] = piece[...]
-        at += piece.shape[0]
-    copies[0].wait()
-    gate_act = jnp.dot(rows[...], gate_here[...], preferred_element_type=jnp.float32)
-    copies[1].wait()
-    up_act = jnp.dot(rows[...], up_here[...], preferred_element_type=jnp.float32)
+    for copy in copies:
+        copy.wait()
+
+
+def load_weights(*weights):
+    hbm = pl.BlockSpec(memory_space=pltpu.HBM)
+    vmem = pl.BlockSpec(memory_space=pltpu.VMEM)
+    return pl.pallas_call(
+        load_kernel,
+        in_specs=[hbm] * 3,
+        out_specs=[vmem] * 3,
+        out_shape=[pltpu.VMEM(w.shape[1:], w.dtype) for w in weights],
+        scratch_shapes=[pltpu.SemaphoreType.DMA((3,))],
+        compiler_params=pltpu.CompilerParams(vmem_limit_bytes=16 * 1024 * 1024),
+    )(*(in_hbm(w) for w in weights))
+
+
+def expert_kernel(first, second, gate, up, down, first_out, second_out, rows, hidden):
+    count = first.shape[0]
+    rows[:count, :] = first[...]
+    rows[count:, :] = second[...]
+    gate_act = jnp.dot(rows[...], gate[...], preferred_element_type=jnp.float32)
+    up_act = jnp.dot(rows[...], up[...], preferred_element_type=jnp.float32)
     hidden[...] = (gate_act / (1.0 + jnp.exp(-gate_act)) * up_act).astype(jnp.bfloat16)
-    copies[2].wait()
-    parts = jnp.dot(hidden[...], down_here[...], preferred_element_type=jnp.float32)
-    at = 0
-    for out in outs:
-        out[...] = parts[at : at + out.shape[0]].astype(jnp.bfloat16)
-        at += out.shape[0]
-
-
-def expert_rows(pieces, gate, up, down):
-    count, width = pieces[0].shape
-    inner = gate.shape[-1]
+    parts = jnp.dot(hidden[...], down[...], preferred_element_type=jnp.float32)
+    first_out[...] = parts[:count].astype(jnp.bfloat16)
+    second_out[...] = parts[count:].astype(jnp.bfloat16)
+
+
+def expert_rows(first, second, weights):
+    count, width = first.shape
+    inner = weights[0].shape[-1]
     vmem = pl.BlockSpec(memory_space=pltpu.VMEM)
-    hbm = pl.BlockSpec(memory_space=pltpu.HBM)
+    here = [pltpu.with_memory_space_constraint(w, pltpu.VMEM) for w in weights]
     return pl.pallas_call(
         expert_kernel,
-        in_specs=[vmem] * 4 + [hbm] * 3,
-        out_specs=[vmem] * 3,
-        out_shape=[
-            jax.ShapeDtypeStruct((n * count, width), jnp.bfloat16) for n in (1, 1, 2)
+        in_specs=[vmem] * 5,
+        out_specs=[vmem] * 2,
+        out_shape=[jax.ShapeDtypeStruct((count, width), jnp.bfloat16)] * 2,
+        scratch_shapes=[
+            pltpu.VMEM((2 * count, width), jnp.bfloat16),
+            pltpu.VMEM((2 * count, inner), jnp.bfloat16),
         ],
-        scratch_shapes=[
-            pltpu.VMEM((4 * count, width), jnp.bfloat16),
-            pltpu.VMEM((4 * count, inner), jnp.bfloat16),
-            pltpu.VMEM((width, inner), jnp.bfloat16),
-            pltpu.VMEM((width, inner), jnp.bfloat16),
-            pltpu.VMEM((inner, width), jnp.bfloat16),
-            pltpu.SemaphoreType.DMA((3,)),
-        ],
-        compiler_params=pltpu.CompilerParams(vmem_limit_bytes=32 * 1024 * 1024),
+        compiler_params=pltpu.CompilerParams(vmem_limit_bytes=24 * 1024 * 1024),
         cost_estimate=pl.CostEstimate(
-            flops=24 * count * width * inner,
-            bytes_accessed=6 * width * inner,
-            transcendentals=4 * count * inner,
+            flops=12 * count * width * inner,
+            bytes_accessed=8 * count * width,
+            transcendentals=2 * count * inner,
         ),
-    )(*pieces, *(in_hbm(w) for w in (gate, up, down)))
+    )(first, second, *here)
 
 
 def added(first, second):
@@ -527,25 +544,19 @@
     return total.astype(jnp.bfloat16)
 
 
-def near_sum_kernel(keep, send, pair, kept, sent):
-    rows = keep.shape[0]
-    kept[...] = added(keep[...], pair[:rows])
-    sent[...] = added(send[...], pair[rows:])
-
-
-def far_sum_kernel(keep, other, out):
-    out[...] = added(keep[...], other[...])
-
-
-def sums(kernel, outputs, *rows):
+def sum_kernel(first, second, out):
+    out[...] = added(first[...], second[...])
+
+
+def summed(first, second):
     vmem = pl.BlockSpec(memory_space=pltpu.VMEM)
     return pl.pallas_call(
-        kernel,
-        in_specs=[vmem] * len(rows),
-        out_specs=[vmem] * outputs,
-        out_shape=[jax.ShapeDtypeStruct(rows[0].shape, jnp.bfloat16)] * outputs,
+        sum_kernel,
+        in_specs=[vmem] * 2,
+        out_specs=vmem,
+        out_shape=jax.ShapeDtypeStruct(first.shape, jnp.bfloat16),
         compiler_params=pltpu.CompilerParams(vmem_limit_bytes=8 * 1024 * 1024),
-    )(*rows)
+    )(first, second)
 
 
 def expert_pairs(
@@ -569,20 +580,24 @@
         capacity,
     )
     far, near = 2, 1
+    weights = load_weights(gate, up, down)
     returned = [None] * experts + [None]
     for k in reversed(range(experts)):
         own = swap(outgoing[k], "ep", k) if k else outgoing[k]
-        across = swap(own, "tp", far)
+        if k == 1:
+            across = swap(swap(outgoing[k], "tp", far), "ep", k)
+        else:
+            across = swap(own, "tp", far)
         beside = swap(own, "tp", near)
         corner = swap(across, "tp", near)
-        pieces = (own, across, beside, corner)
-        keep, send, pair = expert_rows(pieces, gate, up, down)
-        pair = swap(pair, "tp", near)
-        keep, send = sums(near_sum_kernel, 2, keep, send, pair)
-        other = swap(send, "tp", far)
+        keep, near_part = expert_rows(own, beside, weights)
+        send, far_part = expert_rows(across, corner, weights)
+        keep_more = swap(near_part, "tp", near)
+        send_more = swap(far_part, "tp", near)
+        other = swap(summed(send, send_more), "tp", far)
+        keep = summed(keep, keep_more)
         if k:
-            total = sums(far_sum_kernel, 1, keep, other)[0]
-            returned[k] = swap(total, "ep", k)
+            returned[k] = swap(summed(keep, other), "ep", k)
         else:
             returned[0] = keep
             returned[experts] = other

time: 131 us -> 136 us (1.038)
  waiting for transfers between devices: 44.9 us -> 58.9 us
  starting transfers between devices: 47 us -> 39.8 us
  Pallas kernels: 36 us -> 33.3 us
  local copies, waits for them, and re-layouts: 1.51 us -> 2.93 us
    ppermute x29 -> x34, waiting for transfers between devices: 42.2 us -> 51.2 us  [swap(): return lax.ppermute(rows, axis, [(i, i ^ bit) for i in range(size)])]
    ppermute x29 -> x34, starting transfers between devices: 43.2 us -> 36.9 us  [swap(): return lax.ppermute(rows, axis, [(i, i ^ bit) for i in range(size)])]
    ppermute x3, waiting for transfers between devices: 2.71 us -> 7.65 us  [memory_pairs(): earlier.append(lax.ppermute(after, 'ep', [(hop, hop + 1)]))]
    pallas_call x12 -> x21, Pallas kernels: 29.9 us -> 28 us  [the longest x8 18.6 us: expert_rows(): pl.pallas_call(expert_kernel, in_specs=[vmem] * 5, out_specs=[vmem] * 2,...]
    unnamed x18 -> x12, local copies, waits for them, and re-layouts: 1.51 us -> 2.93 us
  transfers between devices with their start and end apart: 32 -> 37, of which waited for: 11 -> 9; matrix products, arithmetic and copies ran while one was open for 0% -> 0% of each run, Pallas kernels for 25% -> 22%
where the time goes in v1:
time: 136 us
  waiting for transfers between devices  58.9 us (43%)
  starting transfers between devices  39.8 us (29%)
  Pallas kernels  33.3 us (24%)
  local copies, waits for them, and re-layouts  2.93 us (2%)
    ppermute x34, waiting for transfers between devices, swap(): return lax.ppermute(rows, axis, [(i, i ^ bit) for i in range(size)])  51.2 us
    ppermute x34, starting transfers between devices, swap(): return lax.ppermute(rows, axis, [(i, i ^ bit) for i in range(size)])  36.9 us
    pallas_call x8, Pallas kernels, expert_rows(): pl.pallas_call(expert_kernel, in_specs=[vmem] * 5, out_specs=[vmem] * 2,...  18.6 us
    ppermute x3, waiting for transfers between devices, memory_pairs(): earlier.append(lax.ppermute(after, 'ep', [(hop, hop + 1)]))  7.65 us
    pallas_call x1, Pallas kernels, load_weights(): pl.pallas_call(load_kernel, in_specs=[hbm] * 3, out_specs=[vmem] * 3, out...  4.23 us
    pallas_call x11, Pallas kernels, summed(): pl.pallas_call(sum_kernel, in_specs=[vmem] * 2, out_specs=vmem, out_shape...  3.29 us
    ppermute x3, starting transfers between devices, memory_pairs(): earlier.append(lax.ppermute(after, 'ep', [(hop, hop + 1)]))  2.93 us
    unnamed x12, local copies, waits for them, and re-layouts  2.93 us
  transfers between devices with their start and end apart: 37, of which 9 were waited for; matrix products, arithmetic and copies ran while one was open for 0% of the time, Pallas kernels for 22%

profile of v1, /device:TPU:0, one launch (start us, length us, event | category | flops | bytes accessed | tf_op | source)
XLA Modules:
  0.0 135.9 jit_solution(2047855444650239126)
XLA Ops:
  0.6 1.8 %shard_map.154 = (f32[128,128]{1,0:T(8,128)S(1)}, bf16[80,2048]{1,0:T(8,128)(2,1)S(1)}, bf16[80,2048]{1,0:T(8,128)(2,1)S(1)}, bf16[80,2048]{1,0:T(8,128)(2,1)S(1)}, bf16[80,2048]{1,0:T(8,128)(2,1)S(1)}) custom-call(s32[1]{0:T(128)} %bitcast.1.refs_0_, bf16[128,2048]{1,0:T(8,128)(2,1)} %refs_1_.3, f32[1,2048]{1,0:T(1,128)} %bitcast.5, s32[2,128]{1,0:T(2,128)} %bitcast.6, ...), custom_call_target="tpu_custom_call" | custom-call | tf_op jit(solution)/shard_map/pallas_call | solution.py:419
  2.4 5.1 %collective-permute-start.25 = (bf16[80,2048]{1,0:T(8,128)(2,1)S(1)}, bf16[80,2048]{1,0:T(8,128)(2,1)S(1)}, u32[]{:S(2)}, u32[]{:S(2)}) collective-permute-start(bf16[80,2048]{1,0:T(8,128)(2,1)S(1)} %get-tuple-element.51), channel_id=1, source_target_pairs={{0,12},{4,8},{8,4},{12,0},{1,13},{5,9},{9,5},{13,1},{2,14},{6,10},... | collective-permute-start | bytes 983048 | tf_op jit(solution)/shard_map/ppermute | solution.py:98
  7.6 1.9 %shard_map.149 = (f32[2,136,128]{2,1,0:T(8,128)S(1)}, f32[2,136,128]{2,1,0:T(8,128)S(1)}, f32[128,256]{1,0:T(8,128)S(1)}, f32[128,128]{1,0:T(8,128)S(1)}) custom-call(bf16[128,256]{1,0:T(8,128)(2,1)} %query.1, bf16[128,256]{1,0:T(8,128)(2,1)} %refs_1_.2, bf16[128,256]{1,0:T(8,128)(2,1)} %refs_2_.1, f32[2,128]{1,0:T(2,128)} %refs_3_.1, f32[2,128]{1,0:T(2,128)} %refs_4_.1, ...), custom_call_target="tpu_custom_call" | custom-call | tf_op jit(solution)/shard_map/pallas_call | solution.py:303
  9.4 1.5 %collective-permute-start = (f32[2,136,128]{2,1,0:T(8,128)S(1)}, f32[2,136,128]{2,1,0:T(8,128)S(1)}, u32[]{:S(2)}, u32[]{:S(2)}) collective-permute-start(f32[2,136,128]{2,1,0:T(8,128)S(1)} %get-tuple-element.32), channel_id=1, source_target_pairs={{0,4},{1,5},{2,6},{3,7},{16,20},{17,21},{18,22},{19,23}} | collective-permute-start | bytes 417800 | tf_op jit(solution)/shard_map/ppermute | solution.py:336
  11.0 7.6 %collective-permute-done.refs_0_ = f32[2,136,128]{2,1,0:T(8,128)S(1)} collective-permute-done((f32[2,136,128]{2,1,0:T(8,128)S(1)}, f32[2,136,128]{2,1,0:T(8,128)S(1)}, u32[]{:S(2)}, u32[]{:S(2)}) %collective-permute-start) | collective-permute-done | bytes 139296 | tf_op jit(solution)/shard_map/ppermute | solution.py:336
  18.7 0.7 collective-permute-start.1
  19.4 1.6 %collective-permute-start.11 = (bf16[80,2048]{1,0:T(8,128)(2,1)S(1)}, bf16[80,2048]{1,0:T(8,128)(2,1)S(1)}, u32[]{:S(2)}, u32[]{:S(2)}) collective-permute-start(bf16[80,2048]{1,0:T(8,128)(2,1)S(1)} %get-tuple-element.41), channel_id=1, source_target_pairs={{0,2},{1,3},{2,0},{3,1},{4,6},{5,7},{6,4},{7,5},{8,10},{9,11},{10,... | collective-permute-start | bytes 983048 | tf_op jit(solution)/shard_map/ppermute | solution.py:98
  20.9 3.1 %collective-permute-start.8 = (bf16[80,2048]{1,0:T(8,128)(2,1)S(1)}, bf16[80,2048]{1,0:T(8,128)(2,1)S(1)}, u32[]{:S(2)}, u32[]{:S(2)}) collective-permute-start(bf16[80,2048]{1,0:T(8,128)(2,1)S(1)} %get-tuple-element.41), channel_id=1, source_target_pairs={{0,4},{4,0},{8,12},{12,8},{1,5},{5,1},{9,13},{13,9},{2,6},{6,2},{1... | collective-permute-start | bytes 983048 | tf_op jit(solution)/shard_map/ppermute | solution.py:98
  24.1 0.8 collective-permute-start.2
  24.9 10.7 %collective-permute-done.17.first = bf16[80,2048]{1,0:T(8,128)(2,1)S(1)} collective-permute-done((bf16[80,2048]{1,0:T(8,128)(2,1)S(1)}, bf16[80,2048]{1,0:T(8,128)(2,1)S(1)}, u32[]{:S(2)}, u32[]{:S(2)}) %collective-permute-start.17) | collective-permute-done | bytes 327712 | tf_op jit(solution)/shard_map/ppermute | solution.py:98
  35.6 1.5 %collective-permute-start.28 = (bf16[80,2048]{1,0:T(8,128)(2,1)S(1)}, bf16[80,2048]{1,0:T(8,128)(2,1)S(1)}, u32[]{:S(2)}, u32[]{:S(2)}) collective-permute-start(bf16[80,2048]{1,0:T(8,128)(2,1)S(1)} %collective-permute-done.25.first), channel_id=1, source_target_pairs={{0,2},{1,3},{2,0},{3,1},{4,6},{5,7},{6,4},{7,5},{8,10},{9,11},{10,... | collective-permute-start | bytes 983048 | tf_op jit(solution)/shard_map/ppermute | solution.py:98
  37.1 4.2 %shard_map.155 = (bf16[2048,896]{1,0:T(8,128)(2,1)S(1)}, bf16[2048,896]{1,0:T(8,128)(2,1)S(1)}, bf16[896,2048]{1,0:T(8,128)(2,1)S(1)}) custom-call(bf16[1,2048,896]{2,1,0:T(8,128)(2,1)} %gate.1, bf16[1,2048,896]{2,1,0:T(8,128)(2,1)} %up.1, bf16[1,896,2048]{2,1,0:T(8,128)(2,1)} %down.1), custom_call_target="tpu_custom_call" | custom-call | tf_op jit(solution)/shard_map/pallas_call | solution.py:497
  41.3 0.8 shard_map.152.own
  42.1 0.6 collective-permute-start.33
  42.7 1.5 %collective-permute-start.20 = (bf16[80,2048]{1,0:T(8,128)(2,1)S(1)}, bf16[80,2048]{1,0:T(8,128)(2,1)S(1)}, u32[]{:S(2)}, u32[]{:S(2)}) collective-permute-start(bf16[80,2048]{1,0:T(8,128)(2,1)S(1)} %collective-permute-done.17.first), channel_id=1, source_target_pairs={{0,2},{1,3},{2,0},{3,1},{4,6},{5,7},{6,4},{7,5},{8,10},{9,11},{10,... | collective-permute-start | bytes 983048 | tf_op jit(solution)/shard_map/ppermute | solution.py:98
  44.2 2.2 %shard_map.168 = (bf16[80,2048]{1,0:T(8,128)(2,1)S(1)}, bf16[80,2048]{1,0:T(8,128)(2,1)S(1)}) custom-call(bf16[80,2048]{1,0:T(8,128)(2,1)S(1)} %collective-permute-done.25.first, bf16[80,2048]{1,0:T(8,128)(2,1)S(1)} %collective-permute-done.26.second, bf16[2048,896]{1,0:T(8,128)(2,1)S(1)} %get-tuple-element.36.gate, ...), custom_call_target="tpu_custom_call" | custom-call | flops 1761607680 | bytes 1310720 | tf_op jit(solution)/shard_map/pallas_call | solution.py:524
  46.5 3.5 %collective-permute-start.12 = (bf16[80,2048]{1,0:T(8,128)(2,1)S(1)}, bf16[80,2048]{1,0:T(8,128)(2,1)S(1)}, u32[]{:S(2)}, u32[]{:S(2)}) collective-permute-start(bf16[80,2048]{1,0:T(8,128)(2,1)S(1)} %collective-permute-done.11), channel_id=1, source_target_pairs={{0,4},{4,0},{8,12},{12,8},{1,5},{5,1},{9,13},{13,9},{2,6},{6,2},{1... | collective-permute-start | bytes 983048 | tf_op jit(solution)/shard_map/ppermute | solution.py:98
  50.0 0.2 collective-permute-start.29
  50.2 2.2 %shard_map.163 = (bf16[80,2048]{1,0:T(8,128)(2,1)S(1)}, bf16[80,2048]{1,0:T(8,128)(2,1)S(1)}) custom-call(bf16[80,2048]{1,0:T(8,128)(2,1)S(1)} %collective-permute-done.17.first, bf16[80,2048]{1,0:T(8,128)(2,1)S(1)} %collective-permute-done.18.second, bf16[2048,896]{1,0:T(8,128)(2,1)S(1)} %get-tuple-element.36.gate, ...), custom_call_target="tpu_custom_call" | custom-call | flops 1761607680 | bytes 1310720 | tf_op jit(solution)/shard_map/pallas_call | solution.py:524
  52.5 0.3 collective-permute-done.33.first
  52.8 6.5 %collective-permute-done.20.first = bf16[80,2048]{1,0:T(8,128)(2,1)S(1)} collective-permute-done((bf16[80,2048]{1,0:T(8,128)(2,1)S(1)}, bf16[80,2048]{1,0:T(8,128)(2,1)S(1)}, u32[]{:S(2)}, u32[]{:S(2)}) %collective-permute-start.20) | collective-permute-done | bytes 327712 | tf_op jit(solution)/shard_map/ppermute | solution.py:98
  59.4 0.5 collective-permute-start.21
  59.9 2.2 %shard_map.158 = (bf16[80,2048]{1,0:T(8,128)(2,1)S(1)}, bf16[80,2048]{1,0:T(8,128)(2,1)S(1)}) custom-call(bf16[80,2048]{1,0:T(8,128)(2,1)S(1)} %collective-permute-done.8.first, bf16[80,2048]{1,0:T(8,128)(2,1)S(1)} %collective-permute-done.9.second, bf16[2048,896]{1,0:T(8,128)(2,1)S(1)} %get-tuple-element.36.gate, ...), custom_call_target="tpu_custom_call" | custom-call | flops 1761607680 | bytes 1310720 | tf_op jit(solution)/shard_map/pallas_call | solution.py:524
  62.1 0.6 collective-permute-start.3
  62.7 2.2 %shard_map.170 = (bf16[80,2048]{1,0:T(8,128)(2,1)S(1)}, bf16[80,2048]{1,0:T(8,128)(2,1)S(1)}) custom-call(bf16[80,2048]{1,0:T(8,128)(2,1)S(1)} %collective-permute-done.28.first, bf16[80,2048]{1,0:T(8,128)(2,1)S(1)} %collective-permute-done.29.second, bf16[2048,896]{1,0:T(8,128)(2,1)S(1)} %get-tuple-element.36.gate, ...), custom_call_target="tpu_custom_call" | custom-call | flops 1761607680 | bytes 1310720 | tf_op jit(solution)/shard_map/pallas_call | solution.py:524
  64.9 0.6 collective-permute-start.27
  65.5 2.2 %shard_map.165 = (bf16[80,2048]{1,0:T(8,128)(2,1)S(1)}, bf16[80,2048]{1,0:T(8,128)(2,1)S(1)}) custom-call(bf16[80,2048]{1,0:T(8,128)(2,1)S(1)} %collective-permute-done.20.first, bf16[80,2048]{1,0:T(8,128)(2,1)S(1)} %collective-permute-done.21.second, bf16[2048,896]{1,0:T(8,128)(2,1)S(1)} %get-tuple-element.36.gate, ...), custom_call_target="tpu_custom_call" | custom-call | flops 1761607680 | bytes 1310720 | tf_op jit(solution)/shard_map/pallas_call | solution.py:524
  67.7 0.1 collective-permute-start.30
  67.8 2.4 %shard_map.160 = (bf16[80,2048]{1,0:T(8,128)(2,1)S(1)}, bf16[80,2048]{1,0:T(8,128)(2,1)S(1)}) custom-call(bf16[80,2048]{1,0:T(8,128)(2,1)S(1)} %collective-permute-done.12.first, bf16[80,2048]{1,0:T(8,128)(2,1)S(1)} %collective-permute-done.13.second, bf16[2048,896]{1,0:T(8,128)(2,1)S(1)} %get-tuple-element.36.gate, ...), custom_call_target="tpu_custom_call" | custom-call | flops 1761607680 | bytes 1310720 | tf_op jit(solution)/shard_map/pallas_call | solution.py:524
  70.2 0.5 collective-permute-start.19
  70.8 0.1 collective-permute-start.22
  70.9 0.4 collective-permute-start.14
  71.3 2.2 %shard_map.173 = (bf16[80,2048]{1,0:T(8,128)(2,1)S(1)}, bf16[80,2048]{1,0:T(8,128)(2,1)S(1)}) custom-call(bf16[80,2048]{1,0:T(8,128)(2,1)S(1)} %collective-permute-done.33.first, bf16[80,2048]{1,0:T(8,128)(2,1)S(1)} %collective-permute-done.34.second, bf16[2048,896]{1,0:T(8,128)(2,1)S(1)} %get-tuple-element.36.gate, ...), custom_call_target="tpu_custom_call" | custom-call | flops 1761607680 | bytes 1310720 | tf_op jit(solution)/shard_map/pallas_call | solution.py:524
  73.5 0.1 collective-permute-start.10
  73.7 0.4 collective-permute-start.35
  74.1 0.1 shard_map.171
  74.2 1.6 %collective-permute-start.31 = (bf16[80,2048]{1,0:T(8,128)(2,1)S(1)}, bf16[80,2048]{1,0:T(8,128)(2,1)S(1)}, u32[]{:S(2)}, u32[]{:S(2)}) collective-permute-start(bf16[80,2048]{1,0:T(8,128)(2,1)S(1)} %shard_map.171), channel_id=1, source_target_pairs={{0,2},{1,3},{2,0},{3,1},{4,6},{5,7},{6,4},{7,5},{8,10},{9,11},{10,... | collective-permute-start | bytes 983048 | tf_op jit(solution)/shard_map/ppermute | solution.py:98
  75.8 0.1 shard_map.166
  75.9 0.6 collective-permute-start.23
  76.4 0.1 shard_map.161
  76.5 1.6 %collective-permute-start.15 = (bf16[80,2048]{1,0:T(8,128)(2,1)S(1)}, bf16[80,2048]{1,0:T(8,128)(2,1)S(1)}, u32[]{:S(2)}, u32[]{:S(2)}) collective-permute-start(bf16[80,2048]{1,0:T(8,128)(2,1)S(1)} %shard_map.161), channel_id=1, source_target_pairs={{0,2},{1,3},{2,0},{3,1},{4,6},{5,7},{6,4},{7,5},{8,10},{9,11},{10,... | collective-permute-start | bytes 983048 | tf_op jit(solution)/shard_map/ppermute | solution.py:98
  78.1 0.5 collective-permute-start.5
  78.6 2.9 %shard_map.156 = (bf16[80,2048]{1,0:T(8,128)(2,1)S(1)}, bf16[80,2048]{1,0:T(8,128)(2,1)}) custom-call(bf16[80,2048]{1,0:T(8,128)(2,1)S(1)} %get-tuple-element.35.first, bf16[80,2048]{1,0:T(8,128)(2,1)S(1)} %collective-permute-done.6.second, bf16[2048,896]{1,0:T(8,128)(2,1)S(1)} %get-tuple-element.36.gate, bf16[2048,896]{1,0:T(8,128)(2,1)S(1)} %get-tuple-element.37.up, ...), custom_call_target="tpu_custom_call" | custom-call | flops 1761607680 | bytes 1310720 | tf_op jit(solution)/shard_map/pallas_call | solution.py:524
  81.6 0.1 shard_map.169.first
  81.6 0.1 shard_map.164.first
  81.7 0.1 shard_map.159.first
  81.8 0.1 shard_map.174
  81.9 2.9 %collective-permute-done.31.second = bf16[80,2048]{1,0:T(8,128)(2,1)S(1)} collective-permute-done((bf16[80,2048]{1,0:T(8,128)(2,1)S(1)}, bf16[80,2048]{1,0:T(8,128)(2,1)S(1)}, u32[]{:S(2)}, u32[]{:S(2)}) %collective-permute-start.31) | collective-permute-done | bytes 327712 | tf_op jit(solution)/shard_map/ppermute | solution.py:98
  84.9 6.9 %collective-permute-done.23.second = bf16[80,2048]{1,0:T(8,128)(2,1)S(1)} collective-permute-done((bf16[80,2048]{1,0:T(8,128)(2,1)S(1)}, bf16[80,2048]{1,0:T(8,128)(2,1)S(1)}, u32[]{:S(2)}, u32[]{:S(2)}) %collective-permute-start.23) | collective-permute-done | bytes 327712 | tf_op jit(solution)/shard_map/ppermute | solution.py:98
  91.9 1.5 %collective-permute-start.36 = (bf16[80,2048]{1,0:T(8,128)(2,1)S(1)}, bf16[80,2048]{1,0:T(8,128)(2,1)S(1)}, u32[]{:S(2)}, u32[]{:S(2)}) collective-permute-start(bf16[80,2048]{1,0:T(8,128)(2,1)S(1)} %shard_map.174), channel_id=1, source_target_pairs={{0,2},{1,3},{2,0},{3,1},{4,6},{5,7},{6,4},{7,5},{8,10},{9,11},{10,... | collective-permute-start | bytes 983048 | tf_op jit(solution)/shard_map/ppermute | solution.py:98
  93.4 0.8 shard_map.167
  94.2 4.7 %collective-permute-done.15.second = bf16[80,2048]{1,0:T(8,128)(2,1)S(1)} collective-permute-done((bf16[80,2048]{1,0:T(8,128)(2,1)S(1)}, bf16[80,2048]{1,0:T(8,128)(2,1)S(1)}, u32[]{:S(2)}, u32[]{:S(2)}) %collective-permute-start.15) | collective-permute-done | bytes 327712 | tf_op jit(solution)/shard_map/ppermute | solution.py:98
  98.9 9.9 %collective-permute-start.32 = (bf16[80,2048]{1,0:T(8,128)(2,1)S(1)}, bf16[80,2048]{1,0:T(8,128)(2,1)S(1)}, u32[]{:S(2)}, u32[]{:S(2)}) collective-permute-start(bf16[80,2048]{1,0:T(8,128)(2,1)S(1)} %shard_map.172), channel_id=1, source_target_pairs={{0,12},{4,8},{8,4},{12,0},{1,13},{5,9},{9,5},{13,1},{2,14},{6,10},... | collective-permute-start | bytes 983048 | tf_op jit(solution)/shard_map/ppermute | solution.py:98
  108.8 0.8 shard_map.162
  109.6 0.6 copy-done.2
  110.2 0.6 copy-done.4
  110.9 0.6 collective-permute-start.16
  111.4 0.8 copy-done.3
  112.3 0.8 copy-done.5
  113.1 1.0 shard_map.153
  114.1 1.1 shard_map.157.refs_1_
  115.1 2.3 %collective-permute-done.32.refs_4_ = bf16[80,2048]{1,0:T(8,128)(2,1)S(1)} collective-permute-done((bf16[80,2048]{1,0:T(8,128)(2,1)S(1)}, bf16[80,2048]{1,0:T(8,128)(2,1)S(1)}, u32[]{:S(2)}, u32[]{:S(2)}) %collective-permute-start.32) | collective-permute-done | bytes 327712 | tf_op jit(solution)/shard_map/ppermute | solution.py:98
  117.4 16.8 %collective-permute-done.24.refs_3_ = bf16[80,2048]{1,0:T(8,128)(2,1)S(1)} collective-permute-done((bf16[80,2048]{1,0:T(8,128)(2,1)}, bf16[80,2048]{1,0:T(8,128)(2,1)S(1)}, u32[]{:S(2)}, u32[]{:S(2)}) %collective-permute-start.24) | collective-permute-done | bytes 327712 | tf_op jit(solution)/shard_map/ppermute | solution.py:98
  134.2 1.7 %shard_map.175 = bf16[128,2048]{1,0:T(8,128)(2,1)} custom-call(f32[128,128]{1,0:T(8,128)S(1)} %get-tuple-element.34.refs_0_, bf16[80,2048]{1,0:T(8,128)(2,1)S(1)} %shard_map.157.refs_1_, bf16[80,2048]{1,0:T(8,128)(2,1)S(1)} %collective-permute-done.16.refs_2_, bf16[80,2048]{1,0:T(8,128)(2,1)S(1)} %collective-permute-done.24.refs_3_, ...), custom_call_target="tpu_custom_call" | custom-call | tf_op jit(solution)/shard_map/pallas_call | solution.py:471
  (49 shorter events, 0.4 us)
Async XLA Ops:
  2.4 21.6 %collective-permute-start.25 = (bf16[80,2048]{1,0:T(8,128)(2,1)S(1)}, bf16[80,2048]{1,0:T(8,128)(2,1)S(1)}, u32[]{:S(2)}, u32[]{:S(2)}) collective-permute-start(bf16[80,2048]{1,0:T(8,128)(2,1)S(1)} %get-tuple-element.51), channel_id=1, source_target_pairs={{0,12},{4,8},{8,4},{12,0},{1,13},{5,9},{9,5},{13,1},{2,14},{6,10},... | collective-permute-start | bytes 983048 | tf_op jit(solution)/shard_map/ppermute | solution.py:98
  9.4 9.2 %collective-permute-start = (f32[2,136,128]{2,1,0:T(8,128)S(1)}, f32[2,136,128]{2,1,0:T(8,128)S(1)}, u32[]{:S(2)}, u32[]{:S(2)}) collective-permute-start(f32[2,136,128]{2,1,0:T(8,128)S(1)} %get-tuple-element.32), channel_id=1, source_target_pairs={{0,4},{1,5},{2,6},{3,7},{16,20},{17,21},{18,22},{19,23}} | collective-permute-start | bytes 417800 | tf_op jit(solution)/shard_map/ppermute | solution.py:336
  10.9 24.7 %collective-permute-start.17 = (bf16[80,2048]{1,0:T(8,128)(2,1)S(1)}, bf16[80,2048]{1,0:T(8,128)(2,1)S(1)}, u32[]{:S(2)}, u32[]{:S(2)}) collective-permute-start(bf16[80,2048]{1,0:T(8,128)(2,1)S(1)} %get-tuple-element.46), channel_id=1, source_target_pairs={{0,8},{4,12},{8,0},{12,4},{1,9},{5,13},{9,1},{13,5},{2,10},{6,14},... | collective-permute-start | bytes 983048 | tf_op jit(solution)/shard_map/ppermute | solution.py:98
  18.7 5.4 %collective-permute-start.1 = (f32[2,136,128]{2,1,0:T(8,128)S(1)}, f32[2,136,128]{2,1,0:T(8,128)S(1)}, u32[]{:S(2)}, u32[]{:S(2)}) collective-permute-start(f32[2,136,128]{2,1,0:T(8,128)S(1)} %shard_map.150), channel_id=1, source_target_pairs={{4,8},{5,9},{6,10},{7,11},{20,24},{21,25},{22,26},{23,27}} | collective-permute-start | bytes 417800 | tf_op jit(solution)/shard_map/ppermute | solution.py:336
  19.4 22.8 %collective-permute-start.11 = (bf16[80,2048]{1,0:T(8,128)(2,1)S(1)}, bf16[80,2048]{1,0:T(8,128)(2,1)S(1)}, u32[]{:S(2)}, u32[]{:S(2)}) collective-permute-start(bf16[80,2048]{1,0:T(8,128)(2,1)S(1)} %get-tuple-element.41), channel_id=1, source_target_pairs={{0,2},{1,3},{2,0},{3,1},{4,6},{5,7},{6,4},{7,5},{8,10},{9,11},{10,... | collective-permute-start | bytes 983048 | tf_op jit(solution)/shard_map/ppermute | solution.py:98
  20.9 21.8 %collective-permute-start.8 = (bf16[80,2048]{1,0:T(8,128)(2,1)S(1)}, bf16[80,2048]{1,0:T(8,128)(2,1)S(1)}, u32[]{:S(2)}, u32[]{:S(2)}) collective-permute-start(bf16[80,2048]{1,0:T(8,128)(2,1)S(1)} %get-tuple-element.41), channel_id=1, source_target_pairs={{0,4},{4,0},{8,12},{12,8},{1,5},{5,1},{9,13},{13,9},{2,6},{6,2},{1... | collective-permute-start | bytes 983048 | tf_op jit(solution)/shard_map/ppermute | solution.py:98
  24.0 20.2 %collective-permute-start.26 = (bf16[80,2048]{1,0:T(8,128)(2,1)S(1)}, bf16[80,2048]{1,0:T(8,128)(2,1)S(1)}, u32[]{:S(2)}, u32[]{:S(2)}) collective-permute-start(bf16[80,2048]{1,0:T(8,128)(2,1)S(1)} %collective-permute-done.25.first), channel_id=1, source_target_pairs={{0,1},{1,0},{2,3},{3,2},{4,5},{5,4},{6,7},{7,6},{8,9},{9,8},{10,11... | collective-permute-start | bytes 983048 | tf_op jit(solution)/shard_map/ppermute | solution.py:98
  24.1 17.2 %copy-start.1 = (bf16[128,256]{1,0:T(8,128)(2,1)S(1)}, bf16[128,256]{1,0:T(8,128)(2,1)}, u32[]{:S(2)}) copy-start(bf16[128,256]{1,0:T(8,128)(2,1)} %query.1) | copy-start | bytes 196612
  24.1 13.0 %collective-permute-start.2 = (f32[2,136,128]{2,1,0:T(8,128)S(1)}, f32[2,136,128]{2,1,0:T(8,128)S(1)}, u32[]{:S(2)}, u32[]{:S(2)}) collective-permute-start(f32[2,136,128]{2,1,0:T(8,128)S(1)} %shard_map.151), channel_id=1, source_target_pairs={{8,12},{9,13},{10,14},{11,15},{24,28},{25,29},{26,30},{27,31}} | collective-permute-start | bytes 417800 | tf_op jit(solution)/shard_map/ppermute | solution.py:336
  35.6 10.9 %collective-permute-start.28 = (bf16[80,2048]{1,0:T(8,128)(2,1)S(1)}, bf16[80,2048]{1,0:T(8,128)(2,1)S(1)}, u32[]{:S(2)}, u32[]{:S(2)}) collective-permute-start(bf16[80,2048]{1,0:T(8,128)(2,1)S(1)} %collective-permute-done.25.first), channel_id=1, source_target_pairs={{0,2},{1,3},{2,0},{3,1},{4,6},{5,7},{6,4},{7,5},{8,10},{9,11},{10,... | collective-permute-start | bytes 983048 | tf_op jit(solution)/shard_map/ppermute | solution.py:98
  37.1 12.9 %collective-permute-start.18 = (bf16[80,2048]{1,0:T(8,128)(2,1)S(1)}, bf16[80,2048]{1,0:T(8,128)(2,1)S(1)}, u32[]{:S(2)}, u32[]{:S(2)}) collective-permute-start(bf16[80,2048]{1,0:T(8,128)(2,1)S(1)} %collective-permute-done.17.first), channel_id=1, source_target_pairs={{0,1},{1,0},{2,3},{3,2},{4,5},{5,4},{6,7},{7,6},{8,9},{9,8},{10,11... | collective-permute-start | bytes 983048 | tf_op jit(solution)/shard_map/ppermute | solution.py:98
  42.1 10.6 %collective-permute-start.33 = (bf16[80,2048]{1,0:T(8,128)(2,1)S(1)}, bf16[80,2048]{1,0:T(8,128)(2,1)S(1)}, u32[]{:S(2)}, u32[]{:S(2)}) collective-permute-start(bf16[80,2048]{1,0:T(8,128)(2,1)S(1)} %get-tuple-element.35.first), channel_id=1, source_target_pairs={{0,2},{1,3},{2,0},{3,1},{4,6},{5,7},{6,4},{7,5},{8,10},{9,11},{10,... | collective-permute-start | bytes 983048 | tf_op jit(solution)/shard_map/ppermute | solution.py:98
  42.7 16.6 %collective-permute-start.20 = (bf16[80,2048]{1,0:T(8,128)(2,1)S(1)}, bf16[80,2048]{1,0:T(8,128)(2,1)S(1)}, u32[]{:S(2)}, u32[]{:S(2)}) collective-permute-start(bf16[80,2048]{1,0:T(8,128)(2,1)S(1)} %collective-permute-done.17.first), channel_id=1, source_target_pairs={{0,2},{1,3},{2,0},{3,1},{4,6},{5,7},{6,4},{7,5},{8,10},{9,11},{10,... | collective-permute-start | bytes 983048 | tf_op jit(solution)/shard_map/ppermute | solution.py:98
  44.2 15.1 %collective-permute-start.9 = (bf16[80,2048]{1,0:T(8,128)(2,1)S(1)}, bf16[80,2048]{1,0:T(8,128)(2,1)S(1)}, u32[]{:S(2)}, u32[]{:S(2)}) collective-permute-start(bf16[80,2048]{1,0:T(8,128)(2,1)S(1)} %collective-permute-done.8.first), channel_id=1, source_target_pairs={{0,1},{1,0},{2,3},{3,2},{4,5},{5,4},{6,7},{7,6},{8,9},{9,8},{10,11... | collective-permute-start | bytes 983048 | tf_op jit(solution)/shard_map/ppermute | solution.py:98
  46.5 15.6 %collective-permute-start.12 = (bf16[80,2048]{1,0:T(8,128)(2,1)S(1)}, bf16[80,2048]{1,0:T(8,128)(2,1)S(1)}, u32[]{:S(2)}, u32[]{:S(2)}) collective-permute-start(bf16[80,2048]{1,0:T(8,128)(2,1)S(1)} %collective-permute-done.11), channel_id=1, source_target_pairs={{0,4},{4,0},{8,12},{12,8},{1,5},{5,1},{9,13},{13,9},{2,6},{6,2},{1... | collective-permute-start | bytes 983048 | tf_op jit(solution)/shard_map/ppermute | solution.py:98
  50.0 12.7 %collective-permute-start.29 = (bf16[80,2048]{1,0:T(8,128)(2,1)S(1)}, bf16[80,2048]{1,0:T(8,128)(2,1)S(1)}, u32[]{:S(2)}, u32[]{:S(2)}) collective-permute-start(bf16[80,2048]{1,0:T(8,128)(2,1)S(1)} %collective-permute-done.28.first), channel_id=1, source_target_pairs={{0,1},{1,0},{2,3},{3,2},{4,5},{5,4},{6,7},{7,6},{8,9},{9,8},{10,11... | collective-permute-start | bytes 983048 | tf_op jit(solution)/shard_map/ppermute | solution.py:98
  52.8 17.4 %collective-permute-start.6 = (bf16[80,2048]{1,0:T(8,128)(2,1)S(1)}, bf16[80,2048]{1,0:T(8,128)(2,1)S(1)}, u32[]{:S(2)}, u32[]{:S(2)}) collective-permute-start(bf16[80,2048]{1,0:T(8,128)(2,1)S(1)} %get-tuple-element.35.first), channel_id=1, source_target_pairs={{0,1},{1,0},{2,3},{3,2},{4,5},{5,4},{6,7},{7,6},{8,9},{9,8},{10,11... | collective-permute-start | bytes 983048 | tf_op jit(solution)/shard_map/ppermute | solution.py:98
  59.3 11.5 %collective-permute-start.34 = (bf16[80,2048]{1,0:T(8,128)(2,1)S(1)}, bf16[80,2048]{1,0:T(8,128)(2,1)S(1)}, u32[]{:S(2)}, u32[]{:S(2)}) collective-permute-start(bf16[80,2048]{1,0:T(8,128)(2,1)S(1)} %collective-permute-done.33.first), channel_id=1, source_target_pairs={{0,1},{1,0},{2,3},{3,2},{4,5},{5,4},{6,7},{7,6},{8,9},{9,8},{10,11... | collective-permute-start | bytes 983048 | tf_op jit(solution)/shard_map/ppermute | solution.py:98
  59.4 5.6 %collective-permute-start.21 = (bf16[80,2048]{1,0:T(8,128)(2,1)S(1)}, bf16[80,2048]{1,0:T(8,128)(2,1)S(1)}, u32[]{:S(2)}, u32[]{:S(2)}) collective-permute-start(bf16[80,2048]{1,0:T(8,128)(2,1)S(1)} %collective-permute-done.20.first), channel_id=1, source_target_pairs={{0,1},{1,0},{2,3},{3,2},{4,5},{5,4},{6,7},{7,6},{8,9},{9,8},{10,11... | collective-permute-start | bytes 983048 | tf_op jit(solution)/shard_map/ppermute | solution.py:98
  62.1 8.7 %collective-permute-start.3 = (bf16[128,256]{1,0:T(8,128)(2,1)S(1)}, bf16[128,256]{1,0:T(8,128)(2,1)S(1)}, u32[]{:S(2)}, u32[]{:S(2)}) collective-permute-start(bf16[128,256]{1,0:T(8,128)(2,1)S(1)} %shard_map.152.own), channel_id=1, source_target_pairs={{0,2},{1,3},{2,0},{3,1},{4,6},{5,7},{6,4},{7,5},{8,10},{9,11},{10,... | collective-permute-start | bytes 196616 | tf_op jit(solution)/shard_map/ppermute | solution.py:98
  62.7 5.0 %collective-permute-start.13 = (bf16[80,2048]{1,0:T(8,128)(2,1)S(1)}, bf16[80,2048]{1,0:T(8,128)(2,1)S(1)}, u32[]{:S(2)}, u32[]{:S(2)}) collective-permute-start(bf16[80,2048]{1,0:T(8,128)(2,1)S(1)} %collective-permute-done.12.first), channel_id=1, source_target_pairs={{0,1},{1,0},{2,3},{3,2},{4,5},{5,4},{6,7},{7,6},{8,9},{9,8},{10,11... | collective-permute-start | bytes 983048 | tf_op jit(solution)/shard_map/ppermute | solution.py:98
  64.9 8.6 %collective-permute-start.27 = (bf16[80,2048]{1,0:T(8,128)(2,1)S(1)}, bf16[80,2048]{1,0:T(8,128)(2,1)S(1)}, u32[]{:S(2)}, u32[]{:S(2)}) collective-permute-start(bf16[80,2048]{1,0:T(8,128)(2,1)S(1)} %get-tuple-element.53), channel_id=1, source_target_pairs={{0,1},{1,0},{2,3},{3,2},{4,5},{5,4},{6,7},{7,6},{8,9},{9,8},{10,11... | collective-permute-start | bytes 983048 | tf_op jit(solution)/shard_map/ppermute | solution.py:98
  67.7 6.0 %collective-permute-start.30 = (bf16[80,2048]{1,0:T(8,128)(2,1)S(1)}, bf16[80,2048]{1,0:T(8,128)(2,1)S(1)}, u32[]{:S(2)}, u32[]{:S(2)}) collective-permute-start(bf16[80,2048]{1,0:T(8,128)(2,1)S(1)} %get-tuple-element.55), channel_id=1, source_target_pairs={{0,1},{1,0},{2,3},{3,2},{4,5},{5,4},{6,7},{7,6},{8,9},{9,8},{10,11... | collective-permute-start | bytes 983048 | tf_op jit(solution)/shard_map/ppermute | solution.py:98
  70.2 6.3 %collective-permute-start.19 = (bf16[80,2048]{1,0:T(8,128)(2,1)S(1)}, bf16[80,2048]{1,0:T(8,128)(2,1)S(1)}, u32[]{:S(2)}, u32[]{:S(2)}) collective-permute-start(bf16[80,2048]{1,0:T(8,128)(2,1)S(1)} %get-tuple-element.48), channel_id=1, source_target_pairs={{0,1},{1,0},{2,3},{3,2},{4,5},{5,4},{6,7},{7,6},{8,9},{9,8},{10,11... | collective-permute-start | bytes 983048 | tf_op jit(solution)/shard_map/ppermute | solution.py:98
  70.8 3.4 %collective-permute-start.22 = (bf16[80,2048]{1,0:T(8,128)(2,1)S(1)}, bf16[80,2048]{1,0:T(8,128)(2,1)S(1)}, u32[]{:S(2)}, u32[]{:S(2)}) collective-permute-start(bf16[80,2048]{1,0:T(8,128)(2,1)S(1)} %get-tuple-element.50), channel_id=1, source_target_pairs={{0,1},{1,0},{2,3},{3,2},{4,5},{5,4},{6,7},{7,6},{8,9},{9,8},{10,11... | collective-permute-start | bytes 983048 | tf_op jit(solution)/shard_map/ppermute | solution.py:98
  70.9 5.0 %collective-permute-start.14 = (bf16[80,2048]{1,0:T(8,128)(2,1)S(1)}, bf16[80,2048]{1,0:T(8,128)(2,1)S(1)}, u32[]{:S(2)}, u32[]{:S(2)}) collective-permute-start(bf16[80,2048]{1,0:T(8,128)(2,1)S(1)} %get-tuple-element.45), channel_id=1, source_target_pairs={{0,1},{1,0},{2,3},{3,2},{4,5},{5,4},{6,7},{7,6},{8,9},{9,8},{10,11... | collective-permute-start | bytes 983048 | tf_op jit(solution)/shard_map/ppermute | solution.py:98
  73.5 4.6 %collective-permute-start.10 = (bf16[80,2048]{1,0:T(8,128)(2,1)S(1)}, bf16[80,2048]{1,0:T(8,128)(2,1)S(1)}, u32[]{:S(2)}, u32[]{:S(2)}) collective-permute-start(bf16[80,2048]{1,0:T(8,128)(2,1)S(1)} %get-tuple-element.43), channel_id=1, source_target_pairs={{0,1},{1,0},{2,3},{3,2},{4,5},{5,4},{6,7},{7,6},{8,9},{9,8},{10,11... | collective-permute-start | bytes 983048 | tf_op jit(solution)/shard_map/ppermute | solution.py:98
  73.7 4.4 %collective-permute-start.35 = (bf16[80,2048]{1,0:T(8,128)(2,1)S(1)}, bf16[80,2048]{1,0:T(8,128)(2,1)S(1)}, u32[]{:S(2)}, u32[]{:S(2)}) collective-permute-start(bf16[80,2048]{1,0:T(8,128)(2,1)S(1)} %get-tuple-element.57), channel_id=1, source_target_pairs={{0,1},{1,0},{2,3},{3,2},{4,5},{5,4},{6,7},{7,6},{8,9},{9,8},{10,11... | collective-permute-start | bytes 983048 | tf_op jit(solution)/shard_map/ppermute | solution.py:98
  74.2 10.6 %collective-permute-start.31 = (bf16[80,2048]{1,0:T(8,128)(2,1)S(1)}, bf16[80,2048]{1,0:T(8,128)(2,1)S(1)}, u32[]{:S(2)}, u32[]{:S(2)}) collective-permute-start(bf16[80,2048]{1,0:T(8,128)(2,1)S(1)} %shard_map.171), channel_id=1, source_target_pairs={{0,2},{1,3},{2,0},{3,1},{4,6},{5,7},{6,4},{7,5},{8,10},{9,11},{10,... | collective-permute-start | bytes 983048 | tf_op jit(solution)/shard_map/ppermute | solution.py:98
  75.9 16.0 %collective-permute-start.23 = (bf16[80,2048]{1,0:T(8,128)(2,1)S(1)}, bf16[80,2048]{1,0:T(8,128)(2,1)S(1)}, u32[]{:S(2)}, u32[]{:S(2)}) collective-permute-start(bf16[80,2048]{1,0:T(8,128)(2,1)S(1)} %shard_map.166), channel_id=1, source_target_pairs={{0,2},{1,3},{2,0},{3,1},{4,6},{5,7},{6,4},{7,5},{8,10},{9,11},{10,... | collective-permute-start | bytes 983048 | tf_op jit(solution)/shard_map/ppermute | solution.py:98
  76.5 22.4 %collective-permute-start.15 = (bf16[80,2048]{1,0:T(8,128)(2,1)S(1)}, bf16[80,2048]{1,0:T(8,128)(2,1)S(1)}, u32[]{:S(2)}, u32[]{:S(2)}) collective-permute-start(bf16[80,2048]{1,0:T(8,128)(2,1)S(1)} %shard_map.161), channel_id=1, source_target_pairs={{0,2},{1,3},{2,0},{3,1},{4,6},{5,7},{6,4},{7,5},{8,10},{9,11},{10,... | collective-permute-start | bytes 983048 | tf_op jit(solution)/shard_map/ppermute | solution.py:98
  78.1 31.5 %collective-permute-start.4 = (bf16[128,256]{1,0:T(8,128)(2,1)S(1)}, bf16[128,256]{1,0:T(8,128)(2,1)S(1)}, u32[]{:S(2)}, u32[]{:S(2)}) collective-permute-start(bf16[128,256]{1,0:T(8,128)(2,1)S(1)} %shard_map.152.own), channel_id=1, source_target_pairs={{0,1},{1,0},{2,3},{3,2},{4,5},{5,4},{6,7},{7,6},{8,9},{9,8},{10,11... | collective-permute-start | bytes 196616 | tf_op jit(solution)/shard_map/ppermute | solution.py:98
  78.1 32.1 %collective-permute-start.5 = (bf16[128,256]{1,0:T(8,128)(2,1)S(1)}, bf16[128,256]{1,0:T(8,128)(2,1)S(1)}, u32[]{:S(2)}, u32[]{:S(2)}) collective-permute-start(bf16[128,256]{1,0:T(8,128)(2,1)S(1)} %collective-permute-done.3.across), channel_id=1, source_target_pairs={{0,1},{1,0},{2,3},{3,2},{4,5},{5,4},{6,7},{7,6},{8,9},{9,8},{10,11... | collective-permute-start | bytes 196616 | tf_op jit(solution)/shard_map/ppermute | solution.py:98
  81.6 29.9 %copy-start = (bf16[1024,512]{1,0:T(8,128)(2,1)S(1)}, bf16[1024,512]{1,0:T(8,128)(2,1)}, u32[]{:S(2)}) copy-start(bf16[1024,512]{1,0:T(8,128)(2,1)} %weight.1) | copy-start | bytes 3145732
  84.8 29.2 %collective-permute-start.7 = (bf16[80,2048]{1,0:T(8,128)(2,1)}, bf16[80,2048]{1,0:T(8,128)(2,1)}, u32[]{:S(2)}, u32[]{:S(2)}) collective-permute-start(bf16[80,2048]{1,0:T(8,128)(2,1)} %get-tuple-element.40), channel_id=1, source_target_pairs={{0,1},{1,0},{2,3},{3,2},{4,5},{5,4},{6,7},{7,6},{8,9},{9,8},{10,11... | collective-permute-start | bytes 983048 | tf_op jit(solution)/shard_map/ppermute | solution.py:98
  91.9 23.3 %collective-permute-start.36 = (bf16[80,2048]{1,0:T(8,128)(2,1)S(1)}, bf16[80,2048]{1,0:T(8,128)(2,1)S(1)}, u32[]{:S(2)}, u32[]{:S(2)}) collective-permute-start(bf16[80,2048]{1,0:T(8,128)(2,1)S(1)} %shard_map.174), channel_id=1, source_target_pairs={{0,2},{1,3},{2,0},{3,1},{4,6},{5,7},{6,4},{7,5},{8,10},{9,11},{10,... | collective-permute-start | bytes 983048 | tf_op jit(solution)/shard_map/ppermute | solution.py:98
  98.9 18.5 %collective-permute-start.32 = (bf16[80,2048]{1,0:T(8,128)(2,1)S(1)}, bf16[80,2048]{1,0:T(8,128)(2,1)S(1)}, u32[]{:S(2)}, u32[]{:S(2)}) collective-permute-start(bf16[80,2048]{1,0:T(8,128)(2,1)S(1)} %shard_map.172), channel_id=1, source_target_pairs={{0,12},{4,8},{8,4},{12,0},{1,13},{5,9},{9,5},{13,1},{2,14},{6,10},... | collective-permute-start | bytes 983048 | tf_op jit(solution)/shard_map/ppermute | solution.py:98
  109.6 0.6 copy-start.2
  110.2 23.9 %collective-permute-start.24 = (bf16[80,2048]{1,0:T(8,128)(2,1)}, bf16[80,2048]{1,0:T(8,128)(2,1)S(1)}, u32[]{:S(2)}, u32[]{:S(2)}) collective-permute-start(bf16[80,2048]{1,0:T(8,128)(2,1)} %shard_map.167), channel_id=1, source_target_pairs={{0,8},{4,12},{8,0},{12,4},{1,9},{5,13},{9,1},{13,5},{2,10},{6,14},... | collective-permute-start | bytes 983048 | tf_op jit(solution)/shard_map/ppermute | solution.py:98
  110.2 0.6 copy-start.4
  110.9 23.3 %collective-permute-start.16 = (bf16[80,2048]{1,0:T(8,128)(2,1)}, bf16[80,2048]{1,0:T(8,128)(2,1)S(1)}, u32[]{:S(2)}, u32[]{:S(2)}) collective-permute-start(bf16[80,2048]{1,0:T(8,128)(2,1)} %shard_map.162), channel_id=1, source_target_pairs={{0,4},{4,0},{8,12},{12,8},{1,5},{5,1},{9,13},{13,9},{2,6},{6,2},{1... | collective-permute-start | bytes 983048 | tf_op jit(solution)/shard_map/ppermute | solution.py:98
  111.4 0.8 copy-start.3
  112.3 0.8 copy-start.5
